TPU v7x, 256 devices: a whole 4x4x8 slice. The times are simulated.
256 devices in a mesh: sp: 16 (over y, x), tp: 16 (over z, core).
Axes of the slice: x: 4, y: 4, z: 8, core: 2. Of those that a mesh axis runs over, the one named last changes fastest.
Arguments:
- latent: bfloat16 [8192, 4096], P(('sp', 'tp')), may hold values from -6 to 6
- context: bfloat16 [512, 4096], P('sp'), may hold values from -6 to 6
- condition: float32 [4096], replicated, may hold values from -6 to 6
- context_condition: float32 [4096], replicated, may hold values from -6 to 6
- modulation: bfloat16 [3, 4096, 4096], P(None, 'sp', 'tp'), may hold values from -0.09375 to 0.09375
- query_weight: bfloat16 [4096, 4096], P(None, 'tp'), as said below
- key_weight: bfloat16 [4096, 4096], P(None, 'tp'), as said below
- value_weight: bfloat16 [4096, 4096], P(None, 'tp'), may hold values from -0.09375 to 0.09375
- lambdas: float32 [16], P('tp'), may hold values from 0.3 to 0.8
- context_lift: float32 [16], P('tp'), may hold values from 1.5 to 3
- head_gain: float32 [256], replicated, may hold values from 0.1 to 1.9
- output_weight: bfloat16 [4096, 4096], P('tp'), may hold values from -0.09375 to 0.09375
Outputs:
- result: bfloat16 [8192, 4096], P(('sp', 'tp'))
Inputs may be any that keep to these rules, and one draw needn't show every extreme that they name: `query_weight`: entries lie within 200 / sqrt(4096) in magnitude. `key_weight`: entries lie within 6 / sqrt(4096) in magnitude.
All inputs are finite; a program needn't handle non-finite values.
Results may differ from a plain program's by a relative error of at most 0.025.
Values may be sent and summed in bfloat16 or wider, within the bound.
A program may use at most 64 MiB of HBM per device.

v0:
```python
import functools
import math

import jax
import jax.numpy as jnp
from jax import lax
from jax.sharding import Mesh
from jax.sharding import PartitionSpec as P

GRID_W = 64
SP = ("sp_0", "sp_1")
SP_TP = ("sp_0", "sp_1", "tp")


ROPE_BASE = 10000.0
EPSILON = 1e-05


def by_axis(shard, axes):
    return functools.reduce(lax.psum, axes, shard)


def from_everyone(shard, axis):
    copies = jnp.broadcast_to(shard, (lax.axis_size(axis), *shard.shape))
    return lax.all_to_all(copies, axis, split_axis=0, concat_axis=0, tiled=True)


def laid_out(pieces, dim):
    pieces = jnp.moveaxis(pieces, 0, dim)
    lengths = pieces.shape
    return pieces.reshape(*lengths[:dim], lengths[dim] * lengths[dim + 1], *lengths[dim + 2 :])


def collect(shard, axis, dim):
    pieces = from_everyone(shard, axis)
    return laid_out(pieces, dim)


def modulate(tokens_in, offset, scaling):
    values = tokens_in.astype(jnp.float32)
    center = jnp.mean(values, axis=-1, keepdims=True)
    spread = jnp.mean(jnp.square(values - center), axis=-1, keepdims=True)
    normed = (values - center) * lax.rsqrt(spread + EPSILON)
    return (normed * (1.0 + scaling) + offset).astype(jnp.bfloat16)


def rotate(tensor, places):
    number, head_count, head_width = tensor.shape
    quarter = head_width // 4
    eighth = head_width // 8
    inverse = ROPE_BASE ** (-jnp.arange(eighth, dtype=jnp.float32) / eighth)
    grid_row = (places // GRID_W).astype(jnp.float32)
    grid_col = (places % GRID_W).astype(jnp.float32)
    angles = jnp.stack([grid_row[:, None] * inverse, grid_col[:, None] * inverse], axis=1)
    cosine = jnp.cos(angles)[:, None, None, :, :]
    sine_table = jnp.sin(angles)[:, None, None, :, :]
    pieces = tensor.reshape(number, head_count, 2, 2, quarter)
    first_half = pieces[..., :eighth]
    second = pieces[..., eighth:]
    turned = jnp.concatenate(
        [first_half * cosine - second * sine_table, second * cosine + first_half * sine_table],
        axis=-1,
    )
    return turned.reshape(number, head_count, head_width)


def absorb(state_in, key_block, queries, lift_term, scale_factor):
    running_max, running_sum, running_out = state_in
    key_count = key_block.shape[0]
    head_count = queries.shape[1]
    head_width = 2 * queries.shape[3]
    local_width = head_count * head_width
    key_part = key_block[:, :local_width].reshape(key_count, head_count, 2, head_width // 2)
    value_part = key_block[:, local_width:].reshape(key_count, head_count, head_width)
    scores = (
        jnp.einsum("qhmd,khmd->mqhk", queries, key_part, preferred_element_type=jnp.float32)
        * scale_factor
        + lift_term
    )
    new_max = jnp.maximum(running_max, jnp.max(scores, axis=-1))
    fading = jnp.exp(running_max - new_max)
    weights = jnp.exp(scores - new_max[..., None])
    new_sum = running_sum * fading + jnp.sum(weights, axis=-1)
    new_out = running_out * fading[..., None] + jnp.einsum(
        "mqhk,khd->mqhd",
        weights.astype(jnp.bfloat16),
        value_part,
        preferred_element_type=jnp.float32,
    )
    return (new_max, new_sum, new_out)


def shards(
    latent,
    context,
    condition,
    context_condition,
    modulation,
    query_weight,
    key_weight,
    value_weight,
    lambdas,
    context_lift,
    head_gain,
    output_weight,
):
    sp_index = lax.axis_index(SP)
    rows_block = modulation.shape[1]
    silu_pair = jax.nn.silu(jnp.stack([condition, context_condition])).astype(jnp.bfloat16)
    own_rows = lax.dynamic_slice_in_dim(silu_pair, sp_index * rows_block, rows_block, 1)
    partial_mod = jnp.einsum(
        "cd,rde->cre", own_rows, modulation, preferred_element_type=jnp.float32
    )
    summed = by_axis(partial_mod, SP)
    mod_vectors = collect(summed, "tp", 2)
    head_count = lambdas.shape[0]
    head_width = query_weight.shape[1] // head_count
    half_width = head_width // 2
    local_width = head_count * head_width
    scale_factor = half_width ** (-0.5)
    normed = modulate(latent, mod_vectors[0, 0], mod_vectors[0, 1])
    projection = jnp.concatenate([query_weight, key_weight, value_weight], axis=1)
    projected = jnp.dot(
        lax.all_gather(normed, "tp", axis=0, tiled=True),
        projection,
        preferred_element_type=jnp.float32,
    ).astype(jnp.bfloat16)
    block_tokens = projected.shape[0]
    places = sp_index * block_tokens + jnp.arange(block_tokens, dtype=jnp.int32)
    queries = rotate(
        projected[:, :local_width]
        .astype(jnp.float32)
        .reshape(block_tokens, head_count, head_width),
        places,
    )
    queries = queries.astype(jnp.bfloat16).reshape(block_tokens, head_count, 2, half_width)
    latent_keys = rotate(
        projected[:, local_width : 2 * local_width]
        .astype(jnp.float32)
        .reshape(block_tokens, head_count, head_width),
        places,
    )
    latent_keys = latent_keys.astype(jnp.bfloat16).reshape(block_tokens, local_width)
    packed = jnp.concatenate([latent_keys, projected[:, 2 * local_width :]], axis=1)
    normed_context = modulate(context, mod_vectors[1, 0], mod_vectors[1, 1])
    own_context = jnp.dot(
        normed_context, projection[:, local_width:], preferred_element_type=jnp.float32
    ).astype(jnp.bfloat16)
    context_packed = collect(own_context, SP, 0)
    initial = (
        jnp.full((2, block_tokens, head_count), -jnp.inf, jnp.float32),
        jnp.zeros((2, block_tokens, head_count), jnp.float32),
        jnp.zeros((2, block_tokens, head_count, head_width), jnp.float32),
    )
    state_now = absorb(initial, context_packed, queries, context_lift[:, None], scale_factor)
    segment = lax.all_gather(packed, SP, axis=0, tiled=True)
    length = segment.shape[0]
    block_len = math.gcd(length, 1024)
    stacked = segment.reshape(length // block_len, block_len, segment.shape[1])

    def one_block(state_step, block_rows):
        return (absorb(state_step, block_rows, queries, 0.0, scale_factor), None)

    running_max, running_sum, running_out = lax.scan(one_block, state_now, stacked)[0]
    means = running_out / running_sum[..., None]
    difference = means[0] - lambdas[None, :, None] * means[1]
    scaled = (
        difference
        * lax.rsqrt(jnp.mean(jnp.square(difference), axis=-1, keepdims=True) + EPSILON)
        * head_gain
    )
    attended = scaled.astype(jnp.bfloat16).reshape(block_tokens, local_width)
    mixture = lax.psum_scatter(
        jnp.dot(attended, output_weight, preferred_element_type=jnp.float32).astype(jnp.bfloat16),
        "tp",
        scatter_dimension=0,
        tiled=True,
    ).astype(jnp.float32)
    return (latent.astype(jnp.float32) + mod_vectors[0, 2] * mixture).astype(jnp.bfloat16)


def solution(mesh):
    split = Mesh(mesh.devices.reshape(4, 4, mesh.shape["tp"]), ("sp_0", "sp_1", "tp"))
    return jax.shard_map(
        shards,
        mesh=split,
        in_specs=(
            P(SP_TP, None),
            P(SP, None),
            P(),
            P(),
            P(None, SP, "tp"),
            P(None, "tp"),
            P(None, "tp"),
            P(None, "tp"),
            P("tp"),
            P("tp"),
            P(),
            P("tp", None),
        ),
        out_specs=P(SP_TP, None),
        check_vma=False,
    )
```

profile of v0, /device:TPU:1, one launch (start us, length us, event | category | flops | bytes accessed | tf_op | source)
XLA Modules:
  0.0 302.9 jit_solution(5398257934742290326)
XLA Ops:
  6.5 1.4 fusion.78
  7.9 9.6 %psum.14 = f32[2,3,256]{2,0,1:T(2,128)S(1)} all-reduce(f32[2,3,256]{2,0,1:T(2,128)S(1)} %fusion.78), channel_id=1, replica_groups=mesh['sp_0'=4,'sp_1'=4,'tp'=16] {'sp_0'}, use_global_device_ids=true, to_apply=%region_0.1 | all-reduce | flops 1536 | bytes 12288 | tf_op jit(solution)/shard_map/psum | solution.py:20
  17.6 8.9 %psum.15 = f32[2,3,256]{2,0,1:T(2,128)S(1)} all-reduce(f32[2,3,256]{2,0,1:T(2,128)S(1)} %psum.14), channel_id=1, replica_groups=mesh['sp_0'=4,'sp_1'=4,'tp'=16] {'sp_1'}, use_global_device_ids=true, to_apply=%region_1.2 | all-reduce | flops 1536 | bytes 12288 | tf_op jit(solution)/shard_map/psum | solution.py:20
  27.2 12.8 %all-to-all-start = ((f32[16,2,3,256]{3,1,2,0:T(2,128)}), f32[16,2,3,256]{3,1,2,0:T(2,128)S(1)}, u32[]{:S(2)}, u32[]{:S(2)}) async-start(f32[16,2,3,256]{3,1,2,0:T(2,128)} %broadcast_in_dim.12), calls=%async_computation | async-start | bytes 196608 | tf_op jit(solution)/shard_map/all_to_all | solution.py:25
  42.4 6.1 %all-to-all-done = f32[16,2,3,256]{3,1,2,0:T(2,128)S(1)} async-done(((f32[16,2,3,256]{3,1,2,0:T(2,128)}), f32[16,2,3,256]{3,1,2,0:T(2,128)S(1)}, u32[]{:S(2)}, u32[]{:S(2)}) %all-to-all-start) | async-done | bytes 98336 | tf_op jit(solution)/shard_map/all_to_all | solution.py:25
  48.6 1.8 fusion.51
  51.0 33.7 %all-gather.3.cloned.1.call-done = bf16[512,4096]{1,0:T(8,128)(2,1)} async-done(((bf16[32,4096]{1,0:T(8,128)(2,1)}), bf16[512,4096]{1,0:T(8,128)(2,1)}) %all-gather.3.cloned.1.call-update) | async-done | bytes 4194320 | tf_op jit(solution)/shard_map/all_gather | solution.py:124
  84.8 7.5 %fusion.31 = bf16[512,768]{1,0:T(8,128)(2,1)S(1)} fusion(bf16[512,4096]{1,0:T(8,128)(2,1)} %all-gather.3.cloned.1.call-done, bf16[4096,256]{1,0:T(8,128)(2,1)} %param.21, bf16[4096,256]{1,0:T(8,128)(2,1)} %param.20, bf16[4096,256]{1,0:T(8,128)(2,1)} %param.19), kind=kOutput, calls=%fused_computation.37 | convolution fusion | flops 3240493056 | bytes 11272192 | tf_op jit(solution)/shard_map/dot_general | solution.py:123
  94.7 1.8 pad_maximum_fusion
  98.8 3.2 %fusion.36 = bf16[32,512]{1,0:T(8,128)(2,1)S(1)} fusion(bf16[4096,256]{1,0:T(8,128)(2,1)} %param.21, bf16[4096,256]{1,0:T(8,128)(2,1)} %param.20, bf16[32,4096]{1,0:T(8,128)(2,1)} %param.15, f32[4096]{0:T(1024)S(1)} %bitcast.171, f32[4096]{0:T(1024)S(1)} %bitcast.172, f32[32]{0:T(128)S(1)} %add_rsqrt_fusion.2, f32[32]{0:T(128)S(1)} %broadcast_multiply_fusion.3), kind=kOutput, calls=%fused_computation.41 | convolution fusion | flops 143409152 | bytes 4522240 | tf_op jit(solution)/shard_map/dot_general | solution.py:146
  102.9 6.5 %all-to-all-start.1 = ((bf16[16,32,512]{2,1,0:T(8,128)(2,1)}), bf16[16,32,512]{2,1,0:T(8,128)(2,1)S(1)}, u32[]{:S(2)}, u32[]{:S(2)}) async-start(bf16[16,32,512]{2,1,0:T(8,128)(2,1)} %broadcast_in_dim.13), calls=%async_computation.1 | async-start | bytes 1048576 | tf_op jit(solution)/shard_map/all_to_all | solution.py:25
  111.0 15.4 %all-to-all-done.1 = bf16[16,32,512]{2,1,0:T(8,128)(2,1)S(1)} async-done(((bf16[16,32,512]{2,1,0:T(8,128)(2,1)}), bf16[16,32,512]{2,1,0:T(8,128)(2,1)S(1)}, u32[]{:S(2)}, u32[]{:S(2)}) %all-to-all-start.1) | async-done | bytes 524320 | tf_op jit(solution)/shard_map/all_to_all | solution.py:25
  127.2 1.8 copy.35
  129.5 1.5 bitcast_reduce_fusion.1
  131.5 1.7 fusion.35
  133.2 41.4 %all-gather.5.cloned.1.call-done = bf16[8192,512]{1,0:T(8,128)(2,1)} async-done(((bf16[512,512]{1,0:T(8,128)(2,1)}), bf16[8192,512]{1,0:T(8,128)(2,1)}) %all-gather.5.cloned.1.call-update) | async-done | bytes 8388624 | tf_op jit(solution)/shard_map/all_gather | solution.py:156
  174.6 54.9 %while.14 = (s32[]{:T(128)}, f32[2,512,1]{1,0,2:T(2,128)S(1)}, f32[2,512,1]{1,0,2:T(2,128)S(1)}, f32[2,512,1,256]{1,3,0,2:T(8,128)}, bf16[8,1024,512]{2,1,0:T(8,...) while((s32[]{:T(128)}, f32[2,512,1]{1,0,2:T(2,128)S(1)}, f32[2,512,1]{1,0,2:T(2,128)S(1)}, ...), condition=%wide.region_11.12_spmd, body=%wide.region_8.11_spmd.sunk | while | flops 814222336 | bytes 33882276 | solution.py:164
  174.6 1.3 constant_dynamic-slice_fusion.2
  175.9 1.3 copy.54
  181.5 1.3 constant_dynamic-slice_fusion.2
  182.8 1.3 copy.54
  188.4 1.3 constant_dynamic-slice_fusion.2
  189.7 1.3 copy.54
  196.5 1.3 copy.54
  203.4 1.3 copy.54
  210.3 1.3 copy.54
  217.1 1.3 copy.54
  224.0 1.3 copy.54
  229.5 1.4 broadcast_divide_fusion
  231.1 3.3 %convolution_convert_fusion = bf16[512,4096]{1,0:T(8,128)(2,1)} fusion(bf16[256,4096]{1,0:T(8,128)(2,1)S(1)} %copy-done, f32[256]{0:T(256)S(1)} %copy-done.7, f32[512]{0:T(512)S(1)} %add_rsqrt_fusion, f32[2,512,1,256]{1,3,0,2:T(8,128)S(1)} %broadcast_divide_fusion, f32[]{:T(128)} %bitcast.145), kind=kOutput, calls=%fused_computation.26 | convolution fusion | flops 1076494336 | bytes 7343108 | tf_op jit(solution)/shard_map/dot_general | solution.py:174
  234.4 60.2 %reduce-scatter.2.cloned.1.call-done = bf16[32,4096]{1,0:T(8,128)(2,1)} async-done(((bf16[512,4096]{1,0:T(8,128)(2,1)}), bf16[32,4096]{1,0:T(8,128)(2,1)}) %reduce-scatter.2.cloned.1.call-update) | async-done | bytes 262160 | tf_op jit(solution)/shard_map/reduce_scatter | solution.py:173
  294.7 1.7 fusion.56
  (156 shorter events, 51.5 us)
Async XLA Ops:
  6.5 224.5 %copy-start = (bf16[256,4096]{1,0:T(8,128)(2,1)S(1)}, bf16[256,4096]{1,0:T(8,128)(2,1)}, u32[]{:S(2)}) copy-start(bf16[256,4096]{1,0:T(8,128)(2,1)} %param.25) | copy-start | bytes 6291460
  27.2 21.3 %all-to-all-start = ((f32[16,2,3,256]{3,1,2,0:T(2,128)}), f32[16,2,3,256]{3,1,2,0:T(2,128)S(1)}, u32[]{:S(2)}, u32[]{:S(2)}) async-start(f32[16,2,3,256]{3,1,2,0:T(2,128)} %broadcast_in_dim.12), calls=%async_computation | async-start | bytes 196608 | tf_op jit(solution)/shard_map/all_to_all | solution.py:25
  40.0 44.7 %all-gather.3.cloned.1.call-start = ((), (), s32[]{:S(2)}) async-start(), calls=%async_computation.3 | async-start | bytes 4456448 | tf_op jit(solution)/shard_map/all_gather | solution.py:124
  50.4 124.2 %all-gather.5.cloned.1.call-start = ((), (), s32[]{:S(2)}) async-start(), calls=%async_computation.4 | async-start | bytes 8912896 | tf_op jit(solution)/shard_map/all_gather | solution.py:156
  102.9 23.5 %all-to-all-start.1 = ((bf16[16,32,512]{2,1,0:T(8,128)(2,1)}), bf16[16,32,512]{2,1,0:T(8,128)(2,1)S(1)}, u32[]{:S(2)}, u32[]{:S(2)}) async-start(bf16[16,32,512]{2,1,0:T(8,128)(2,1)} %broadcast_in_dim.13), calls=%async_computation.1 | async-start | bytes 1048576 | tf_op jit(solution)/shard_map/all_to_all | solution.py:25
  109.5 185.2 %reduce-scatter.2.cloned.1.call-start = ((), (), s32[]{:S(2)}) async-start(), calls=%async_computation.5 | async-start | bytes 4456448 | tf_op jit(solution)/shard_map/reduce_scatter | solution.py:173
  126.4 2.6 copy-start.5
  129.3 2.1 copy-start.6
  174.6 56.4 %copy-start.7 = (f32[256]{0:T(256)S(1)}, f32[256]{0:T(256)}, u32[]{:S(2)}) copy-start(f32[256]{0:T(256)} %param.24) | copy-start | bytes 3076
  177.3 2.0 copy-start.1
  177.3 2.0 copy-start.2
  180.4 1.1 copy-start.3
  184.1 2.0 copy-start.1
  184.1 2.0 copy-start.2
  187.3 1.1 copy-start.3
  191.0 2.0 copy-start.1
  191.0 2.0 copy-start.2
  194.2 1.1 copy-start.3
  197.8 2.0 copy-start.1
  197.8 2.0 copy-start.2
  201.0 1.1 copy-start.3
  204.7 2.0 copy-start.1
  204.7 2.0 copy-start.2
  207.9 1.1 copy-start.3
  211.6 2.0 copy-start.1
  211.6 2.0 copy-start.2
  214.8 1.1 copy-start.3
  218.4 2.0 copy-start.1
  218.4 2.0 copy-start.2
  225.3 2.0 copy-start.1
  225.3 2.0 copy-start.2
  231.1 63.6 %copy-start.4 = (bf16[32,4096]{1,0:T(8,128)(2,1)S(1)}, bf16[32,4096]{1,0:T(8,128)(2,1)}, u32[]{:S(2)}) copy-start(bf16[32,4096]{1,0:T(8,128)(2,1)} %param.14) | copy-start | bytes 786436
  (2 other events, 2.1 us)
Sparse Core Ops, SparseCore 0:
  50.5 34.1 all-gather.2
  96.6 77.9 all-gather.4
  234.5 60.0 reduce-scatter.1
where the time goes:
time: 306 us; the launch traced here: 303 us
  waiting for transfers between devices  157 us (51%)
  local copies, waits for them, and re-layouts  39.2 us (13%)
  matrix products  33.8 us (11%)
  starting transfers between devices  19.7 us (6%)
  other arithmetic  19.6 us (6%)
  blocking collectives  18.6 us (6%)
  between operations  14.6 us (5%)
    reduce_scatter x1, waiting for transfers between devices, shards(): lax.psum_scatter(jnp.dot(attended, output_weight, preferred_element_type=...  60.2 us
    all_gather x1, waiting for transfers between devices, shards(): segment = lax.all_gather(packed, SP, axis=0, tiled=True)  41.4 us
    all_gather x1, waiting for transfers between devices, shards(): lax.all_gather(normed, 'tp', axis=0, tiled=True)  33.7 us
    all_to_all x2, waiting for transfers between devices, from_everyone(): return lax.all_to_all(copies, axis, split_axis=0, concat_axis=0, tiled=True)  21.5 us
    dynamic_slice x16, local copies, waits for them, and re-layouts, shards(): lax.scan(one_block, state_now, stacked)[0]  20.8 us
    all_to_all x2, starting transfers between devices, from_everyone(): return lax.all_to_all(copies, axis, split_axis=0, concat_axis=0, tiled=True)  19.4 us
    psum x2, blocking collectives, by_axis(): return functools.reduce(lax.psum, axes, shard)  18.6 us
    slice x10, local copies, waits for them, and re-layouts, absorb(): key_block[:, :local_width]  12.4 us
  transfers between devices with their start and end apart: 5, of which 5 were waited for; matrix products, arithmetic and copies ran while one was open for 5% of the time, Pallas kernels for 0%

commit v1 on v0

v1 whole, which is shorter than its diff:
```python
import functools
import math

import jax
import jax.numpy as jnp
import numpy as np
from jax import lax
from jax.experimental import pallas as pl
from jax.experimental.pallas import tpu as pltpu
from jax.sharding import Mesh
from jax.sharding import PartitionSpec as P

MESH = pl.DeviceIdType.MESH
F32 = jnp.float32
BF16 = jnp.bfloat16

WIDTH = 4096
GRID_W = 64
ROPE_BASE = 10000.0
EPSILON = 1e-05
HEAD = 256
PART = 128
LOG2E = math.log2(math.e)
SCALE2 = PART ** (-0.5) * LOG2E
ROWS = 512
OWN = 32
CTX = 32
MEMBERS = 4
LAT_KEYS = MEMBERS * ROWS
KEYS = LAT_KEYS + MEMBERS * CTX
TILE = 256
OFFSET = (0, -1, 1, -2, 2, -3, 3, 4)
PASSES = ((0,), (1, 2), (3, 4), (5, 6), (7,))


def rope_tables():
    quarter = PART // 2
    eighth = PART // 4
    inverse = np.float32(ROPE_BASE) ** (-np.arange(eighth, dtype=np.float32) / np.float32(eighth))
    inverse = inverse.astype(np.float32)
    sign = np.concatenate([-np.ones(eighth), np.ones(eighth)]).astype(np.float32)

    def pair(count):
        angles = np.arange(count, dtype=np.float32)[:, None] * np.concatenate([inverse, inverse])
        angles = angles.astype(np.float32).astype(np.float64)
        return np.cos(angles).astype(np.float32), (np.sin(angles) * sign).astype(np.float32)

    row_cos, row_sin = pair(8192 // GRID_W)
    col_cos, col_sin = pair(GRID_W)
    none = np.zeros_like(row_cos)
    row_cos, row_sin = (np.concatenate([t, none], axis=1) for t in (row_cos, row_sin))
    none = np.zeros_like(col_cos)
    col_cos, col_sin = (np.concatenate([none, t], axis=1) for t in (col_cos, col_sin))
    half = GRID_W // 2
    both = [np.stack([t, np.concatenate([t[half:], t[:half]])]) for t in (col_cos, col_sin)]
    return row_cos, row_sin, both[0], both[1]


def body(
    latent,
    context,
    condition,
    context_condition,
    modulation,
    query_weight,
    key_weight,
    value_weight,
    lambdas,
    context_lift,
    head_gain,
    output_weight,
    row_cos,
    row_sin,
    col_cos,
    col_sin,
    result,
    gx,
    ctx,
    modw,
    weights,
    xn,
    mod_y,
    mod_x,
    mod_all,
    raw,
    qs,
    kv,
    outs,
    outs_in,
    stats,
    stats_in,
    att,
    att_in,
    wout,
    part,
    sum_out,
    sum_in,
    load_sem,
    xs,
    xr,
    ps,
    pr,
    ms,
    mr,
    zs,
    zr,
    fs,
    fr,
    qsem_s,
    qsem_r,
    ksem_s,
    ksem_r,
    csem_s,
    csem_r,
    osem_s,
    osem_r,
    tsem_s,
    tsem_r,
    asem,
    wsem,
    rs,
    rr,
):
    y, x, z, c = (lax.axis_index(a) for a in ("y", "x", "z", "c"))
    sp = y * 4 + x
    waits = []

    def remote(src, dst, send, recv, to):
        return pltpu.make_async_remote_copy(
            src_ref=src, dst_ref=dst, send_sem=send, recv_sem=recv, device_id=to, device_id_type=MESH
        )

    def go(copy):
        copy.start()
        waits.append(copy)

    partner = {"c": 1 - c}

    def on_y(d):
        return {"y": lax.rem(y + d, 4)}

    def on_x(d):
        return {"x": lax.rem(x + d, 4)}

    def on_z(d):
        return {"z": lax.rem(z + d + 8, 8)}

    def on_queries(d):
        return {"y": lax.rem(y + d * c, 4), "x": lax.rem(x + d * (1 - c), 4)}

    def on_keys(d):
        return {"y": lax.rem(y + d * (1 - c), 4), "x": lax.rem(x + d * c, 4)}

    loads = [
        pltpu.make_async_copy(latent, gx.at[0, pl.ds(0, OWN)], load_sem.at[0]),
        pltpu.make_async_copy(modulation, modw, load_sem.at[1]),
        pltpu.make_async_copy(context, ctx, load_sem.at[2]),
        pltpu.make_async_copy(query_weight, weights.at[0], load_sem.at[3]),
        pltpu.make_async_copy(key_weight, weights.at[1], load_sem.at[4]),
        pltpu.make_async_copy(value_weight, weights.at[2], load_sem.at[5]),
        pltpu.make_async_copy(output_weight, wout.at[0], load_sem.at[6]),
    ]
    for load in loads:
        load.start()

    barrier = pltpu.get_barrier_semaphore()
    peers = [on_y(d) for d in (1, 2, 3)] + [on_x(d) for d in (1, 2, 3)]
    peers += [on_z(d) for d in range(1, 8)] + [partner]
    for peer in peers:
        pl.semaphore_signal(barrier, inc=1, device_id=peer, device_id_type=MESH)
    pl.semaphore_wait(barrier, len(peers))

    def ring_slot(way, k):
        return 0 if k == 0 else 7 if k == 4 else 2 * k - 1 if way == 0 else 2 * k

    def ring_copy(way, k, h):
        rows = pl.ds(16 * h, 16)
        return remote(
            gx.at[ring_slot(way, k - 1), rows],
            gx.at[ring_slot(way, k), rows],
            xs.at[way, k - 1, h],
            xr.at[way, k - 1, h],
            on_z(1 if way == 0 else -1),
        )

    def across(slot, h):
        return remote(
            gx.at[slot, pl.ds(16 * h, 16)],
            gx.at[slot, pl.ds(OWN + 16 * h, 16)],
            ps.at[slot, h],
            pr.at[slot, h],
            partner,
        )

    def relay(k, turn):
        for way in (0, 1):
            h = turn if way == 0 else 1 - turn
            if k == 4 and turn == 1:
                continue
            ring_copy(way, k, h).wait_recv()
            if k < 3 or (k == 3 and turn == 0):
                go(ring_copy(way, k + 1, h))
            go(across(ring_slot(way, k), h))

    loads[0].wait()
    for turn in (0, 1):
        for way in (0, 1):
            go(ring_copy(way, 1, turn if way == 0 else 1 - turn))
    for h in (0, 1):
        go(across(0, h))

    def silu_rows(ref):
        halves = [ref[pl.ds(2 * sp + i, 1), :] for i in (0, 1)]
        v = jnp.concatenate(halves, axis=1)
        return (v / (1.0 + jnp.exp(-v))).astype(BF16).astype(F32)

    own = silu_rows(condition)
    other = silu_rows(context_condition)
    at_row = lax.broadcasted_iota(jnp.int32, (16, 256), 0)
    loads[1].wait()
    partial = jnp.zeros((16, 256), F32)
    for r in range(3):
        lhs = jnp.where(at_row == 2 * r, own, jnp.where(at_row == 2 * r + 1, other, 0.0))
        partial += jnp.dot(lhs.astype(BF16), modw[r], preferred_element_type=F32)
    mod_y[0] = partial[:8]

    def mod_copy(buf, stage, d, to):
        return remote(buf.at[0], buf.at[4 - d], ms.at[stage, d], mr.at[stage, 4 - d], to)

    for d in (2, 1, 3):
        go(mod_copy(mod_y, 0, d, on_y(d)))
    for d in (2, 1, 3):
        mod_copy(mod_y, 0, d, on_y(d)).wait_recv()
    mod_x[0] = (mod_y[0] + mod_y[1]) + (mod_y[2] + mod_y[3])
    for d in (2, 1, 3):
        go(mod_copy(mod_x, 1, d, on_x(d)))
    for d in (2, 1, 3):
        mod_copy(mod_x, 1, d, on_x(d)).wait_recv()
    mod_all[z, c] = (mod_x[0] + mod_x[1]) + (mod_x[2] + mod_x[3])
    for d in (4, 3, 5, 2, 6, 1, 7):
        go(remote(mod_all.at[z, c], mod_all.at[z, c], zs.at[d], zr.at[8 - d], on_z(d)))
    go(remote(mod_all.at[z, c], mod_all.at[z, c], fs.at[0], fr.at[0], partner))
    relay(1, 0)
    relay(1, 1)
    for d in range(1, 8):
        there = lax.rem(z + d, 8)
        slab = mod_all.at[there, c]
        remote(slab, slab, zs.at[d], zr.at[d], on_z(d)).wait_recv()
        go(remote(slab, slab, fs.at[d], fr.at[d], partner))
    relay(2, 0)
    for d in range(8):
        slab = mod_all.at[lax.rem(z + d, 8), 1 - c]
        remote(slab, slab, fs.at[d], fr.at[d], partner).wait_recv()

    def normalize(src, dst_row, which, groups):
        def group(g, carry):
            v = src[pl.ds(pl.multiple_of(g * 16, 16), 16), :].astype(F32)
            center = jnp.mean(v, axis=-1, keepdims=True)
            v = v - center
            spread = jnp.mean(jnp.square(v), axis=-1, keepdims=True)
            inverse = lax.rsqrt(spread + EPSILON)
            for t in range(16):
                cols = slice(t * 256, (t + 1) * 256)
                offset = mod_all[t // 2, t % 2, which : which + 1, :]
                scaling = mod_all[t // 2, t % 2, 2 + which : 3 + which, :]
                done = (v[:, cols] * inverse) * (1.0 + scaling) + offset
                xn[pl.ds(pl.multiple_of(dst_row + g * 16, 16), 16), cols] = done.astype(BF16)
            return carry

        lax.fori_loop(0, groups, group, 0)

    lane = lax.broadcasted_iota(jnp.int32, (64, PART), 1)
    low = lax.rem(lane, 64) < 32

    def project(count):
        def one(g, carry):
            raw[g, pl.ds(0, count)] = jnp.dot(
                xn[pl.ds(0, count), :], weights[g], preferred_element_type=F32
            ).astype(BF16)
            return carry

        lax.fori_loop(0, 3, one, 0)

    def step(p):
        slots = PASSES[p]
        for i, slot in enumerate(slots):
            normalize(gx.at[slot], 64 * i, 0, 4)
        count = 64 * len(slots)
        if p == 0:
            loads[2].wait()
            normalize(ctx, 64, 1, 2)
            count += CTX
            for load in loads[3:6]:
                load.wait()
        project(count)
        for i, slot in enumerate(slots):
            line = sp * 8 + lax.rem(z + OFFSET[slot] + 8, 8)
            cosine = col_cos[c] + row_cos[pl.ds(line, 1), :]
            sine = col_sin[c] + row_sin[pl.ds(line, 1), :]
            base = 64 * slot
            for g in (0, 1):
                for m in (0, 1):
                    cols = slice(m * PART, (m + 1) * PART)
                    a = raw[g, 64 * i : 64 * i + 64, cols].astype(F32)
                    swapped = jnp.where(low, pltpu.roll(a, PART - 32, 1), pltpu.roll(a, 32, 1))
                    turned = (a * cosine + swapped * sine).astype(BF16)
                    if g == 0:
                        qs[0, base : base + 64, cols] = turned
                    else:
                        kv[base : base + 64, cols] = turned
            kv[base : base + 64, HEAD : 2 * HEAD] = raw[2, 64 * i : 64 * i + 64, :]
        if p == 0:
            kv[LAT_KEYS : LAT_KEYS + CTX, 0:HEAD] = raw[1, 64 : 64 + CTX, :]
            kv[LAT_KEYS : LAT_KEYS + CTX, HEAD : 2 * HEAD] = raw[2, 64 : 64 + CTX, :]
        for d in (2, 1, 3):
            go(query_copy(p, d))
            go(key_copy(p, d))
            if p == 0:
                go(context_copy(d))

    def rows_of(p):
        return 64 * PASSES[p][0], 64 * len(PASSES[p])

    def query_copy(p, d):
        start, count = rows_of(p)
        return remote(
            qs.at[0, pl.ds(start, count)],
            qs.at[4 - d, pl.ds(start, count)],
            qsem_s.at[p, d],
            qsem_r.at[p, 4 - d],
            on_queries(d),
        )

    def key_copy(p, d):
        start, count = rows_of(p)
        return remote(
            kv.at[pl.ds(start, count)],
            kv.at[pl.ds((4 - d) * ROWS + start, count)],
            ksem_s.at[p, d],
            ksem_r.at[p, 4 - d],
            on_keys(d),
        )

    def context_copy(d):
        return remote(
            kv.at[pl.ds(LAT_KEYS, CTX)],
            kv.at[pl.ds(LAT_KEYS + (4 - d) * CTX, CTX)],
            csem_s.at[d],
            csem_r.at[4 - d],
            on_keys(d),
        )

    def slots_in(slots, halves=(0, 1)):
        for slot in slots:
            for h in halves:
                across(slot, h).wait_recv()

    slots_in(PASSES[0])
    step(0)
    relay(2, 1)
    slots_in(PASSES[1])
    step(1)
    relay(3, 0)
    relay(3, 1)
    slots_in(PASSES[2])
    step(2)
    relay(4, 0)
    slots_in(PASSES[3])
    step(3)
    slots_in(PASSES[4])
    step(4)
    loads[6].wait()
    go(remote(wout.at[0], wout.at[1], wsem.at[0], wsem.at[1], partner))

    for p in range(5):
        for d in (1, 2, 3):
            query_copy(p, d).wait_recv()
            key_copy(p, d).wait_recv()
    for d in (1, 2, 3):
        context_copy(d).wait_recv()

    lift = context_lift[0] * LOG2E
    column = lax.broadcasted_iota(jnp.int32, (TILE, PART), 1)

    def out_copies(j, half):
        rows = pl.ds(pl.multiple_of(half * TILE, TILE), TILE)
        to = on_queries(j)
        return (
            remote(
                outs.at[j, rows],
                outs_in.at[lax.rem(4 - j, 4), rows],
                osem_s.at[j, half],
                osem_r.at[lax.rem(4 - j, 4), half],
                to,
            ),
            remote(
                stats.at[j, half],
                stats_in.at[lax.rem(4 - j, 4), half],
                tsem_s.at[j, half],
                tsem_r.at[lax.rem(4 - j, 4), half],
                to,
            ),
        )

    def attend(i, carry):
        j = 3 - lax.div(i, 2)
        half = lax.rem(i, 2)
        start = pl.multiple_of(half * TILE, TILE)
        found = []
        for m in (0, 1):
            cols = slice(m * PART, (m + 1) * PART)
            q = qs[j, pl.ds(start, TILE), cols]
            s = lax.dot_general(
                q, kv[:, cols], (((1,), (1,)), ((), ())), preferred_element_type=F32
            )
            near = s[:, :LAT_KEYS]
            far = s[:, LAT_KEYS:] * SCALE2 + lift
            peak = jnp.maximum(
                jnp.max(near, axis=1, keepdims=True) * SCALE2, jnp.max(far, axis=1, keepdims=True)
            )
            near = jnp.exp2(near * SCALE2 - peak)
            far = jnp.exp2(far - peak)
            total = jnp.sum(near, axis=1, keepdims=True) + jnp.sum(far, axis=1, keepdims=True)
            o = jnp.dot(
                near.astype(BF16), kv[:LAT_KEYS, HEAD : 2 * HEAD], preferred_element_type=F32
            ) + jnp.dot(
                far.astype(BF16), kv[LAT_KEYS:, HEAD : 2 * HEAD], preferred_element_type=F32
            )
            outs[j, pl.ds(start, TILE), m * HEAD : (m + 1) * HEAD] = (o / total).astype(BF16)
            found += [peak, total]
        table = jnp.where(
            column == 0,
            found[0],
            jnp.where(column == 1, found[1], jnp.where(column == 2, found[2], found[3])),
        )
        stats[j, half] = table.T[:8, :]

        @pl.when(j > 0)
        def _():
            for copy in out_copies(j, half):
                copy.start()

        return carry

    lax.fori_loop(0, 8, attend, 0)

    for half in (0, 1):
        for j in (3, 2, 1):
            for copy in out_copies(j, half):
                copy.wait_recv()
        rows = pl.ds(half * TILE, TILE)
        tables = [stats[0, half]] + [stats_in[j, half] for j in (1, 2, 3)]
        turned = jnp.concatenate(tables + [jnp.zeros((96, TILE), F32)], axis=0).T
        means = []
        for m in (0, 1):
            peaks = [turned[:, 8 * j + 2 * m : 8 * j + 2 * m + 1] for j in range(4)]
            totals = [turned[:, 8 * j + 2 * m + 1 : 8 * j + 2 * m + 2] for j in range(4)]
            top = jnp.maximum(jnp.maximum(peaks[0], peaks[1]), jnp.maximum(peaks[2], peaks[3]))
            shares = [t * jnp.exp2(p - top) for p, t in zip(peaks, totals)]
            whole = (shares[0] + shares[1]) + (shares[2] + shares[3])
            cols = slice(m * HEAD, (m + 1) * HEAD)
            acc = outs[0, rows, cols].astype(F32) * (shares[0] / whole)
            for j in (1, 2, 3):
                acc += outs_in[j, rows, cols].astype(F32) * (shares[j] / whole)
            means.append(acc)
        difference = means[0] - lambdas[0] * means[1]
        spread = jnp.mean(jnp.square(difference), axis=1, keepdims=True)
        gain = jnp.concatenate([head_gain[0:1, :], head_gain[1:2, :]], axis=1)
        scaled = difference * lax.rsqrt(spread + EPSILON) * gain
        att[4 * half : 4 * half + 4] = scaled.astype(BF16).reshape(4, 2, OWN, HEAD)

    swap = remote(att.at[:, 1], att_in, asem.at[0], asem.at[1], partner)
    go(swap)
    swap.wait_recv()
    remote(wout.at[0], wout.at[1], wsem.at[0], wsem.at[1], partner).wait_recv()

    mine = att[:, 0].reshape(8 * OWN, HEAD)
    theirs = att_in[...].reshape(8 * OWN, HEAD)

    def multiply(n, carry):
        cols = pl.ds(pl.multiple_of(n * 512, 512), 512)
        got = jnp.dot(mine, wout[0, :, cols], preferred_element_type=F32)
        got += jnp.dot(theirs, wout[1, :, cols], preferred_element_type=F32)
        part[:, :, cols] = got.reshape(8, OWN, 512)
        return carry

    lax.fori_loop(0, 8, multiply, 0)

    def sum_slot(way, t):
        return 7 if t == 1 else 2 * (5 - t) if way == 0 else 2 * (5 - t) - 1

    def sum_copy(way, t, h):
        return remote(
            sum_out.at[way, t - 1, h],
            sum_in.at[way, t - 1, h],
            rs.at[way, t - 1, h],
            rr.at[way, t - 1, h],
            on_z(1 if way == 0 else -1),
        )

    def send_sum(way, t, h, add):
        slot = sum_slot(way, t)
        for n in range(4):
            cols = slice(n * 1024, (n + 1) * 1024)
            total = part[slot, 16 * h : 16 * h + 16, cols]
            if add:
                total = total + sum_in[way, t - 2, h, :, cols].astype(F32)
            sum_out[way, t - 1, h, :, cols] = total.astype(BF16)
        go(sum_copy(way, t, h))

    for way in (0, 1):
        send_sum(way, 1, way, False)
    for way in (0, 1):
        send_sum(way, 2, 1 - way, False)
    for t, turn in ((2, 0), (3, 1), (3, 0), (4, 1), (4, 0)):
        for way in (0, 1):
            h = turn if way == 0 else 1 - turn
            sum_copy(way, t - 1, h).wait_recv()
            send_sum(way, t, h, True)
    for turn in (1, 0):
        for way in (0, 1):
            sum_copy(way, 4, turn if way == 0 else 1 - turn).wait_recv()
    for h in (0, 1):
        rows = slice(16 * h, 16 * h + 16)
        for t in range(16):
            cols = slice(t * 256, (t + 1) * 256)
            mixture = part[0, rows, cols] + (
                sum_in[0, 3, h, :, cols].astype(F32) + sum_in[1, 3, h, :, cols].astype(F32)
            )
            gate = mod_all[t // 2, t % 2, 4:5, :]
            result[rows, cols] = (gx[0, rows, cols].astype(F32) + gate * mixture).astype(BF16)

    for copy in waits:
        copy.wait_send()
    for j in (1, 2, 3):
        for half in (0, 1):
            for copy in out_copies(j, half):
                copy.wait_send()


def shards(*args):
    (
        latent,
        context,
        condition,
        context_condition,
        modulation,
        query_weight,
        key_weight,
        value_weight,
        lambdas,
        context_lift,
        head_gain,
        output_weight,
    ) = args
    anywhere = pl.BlockSpec(memory_space=pl.ANY)
    inside = pl.BlockSpec(memory_space=pltpu.VMEM)
    scalar = pl.BlockSpec(memory_space=pltpu.SMEM)
    tables = rope_tables()
    dma = pltpu.SemaphoreType.DMA
    scratch = [
        pltpu.VMEM((8, 64, WIDTH), BF16),
        pltpu.VMEM((CTX, WIDTH), BF16),
        pltpu.VMEM((3, 256, 256), BF16),
        pltpu.VMEM((3, WIDTH, HEAD), BF16),
        pltpu.VMEM((128, WIDTH), BF16),
        pltpu.VMEM((4, 8, 256), F32),
        pltpu.VMEM((4, 8, 256), F32),
        pltpu.VMEM((8, 2, 8, 256), F32),
        pltpu.VMEM((3, 128, HEAD), BF16),
        pltpu.VMEM((4, ROWS, HEAD), BF16),
        pltpu.VMEM((KEYS, 2 * HEAD), BF16),
        pltpu.VMEM((4, ROWS, 2 * HEAD), BF16),
        pltpu.VMEM((4, ROWS, 2 * HEAD), BF16),
        pltpu.VMEM((4, 2, 8, TILE), F32),
        pltpu.VMEM((4, 2, 8, TILE), F32),
        pltpu.VMEM((8, 2, OWN, HEAD), BF16),
        pltpu.VMEM((8, OWN, HEAD), BF16),
        pltpu.VMEM((2, HEAD, WIDTH), BF16),
        pltpu.VMEM((8, OWN, WIDTH), F32),
        pltpu.VMEM((2, 4, 2, 16, WIDTH), BF16),
        pltpu.VMEM((2, 4, 2, 16, WIDTH), BF16),
        dma((7,)),
        dma((2, 4, 2)),
        dma((2, 4, 2)),
        dma((8, 2)),
        dma((8, 2)),
        dma((2, 4)),
        dma((2, 4)),
        dma((8,)),
        dma((8,)),
        dma((8,)),
        dma((8,)),
        dma((5, 4)),
        dma((5, 4)),
        dma((5, 4)),
        dma((5, 4)),
        dma((4,)),
        dma((4,)),
        dma((4, 2)),
        dma((4, 2)),
        dma((4, 2)),
        dma((4, 2)),
        dma((2,)),
        dma((2,)),
        dma((2, 4, 2)),
        dma((2, 4, 2)),
    ]
    return pl.pallas_call(
        body,
        out_shape=jax.ShapeDtypeStruct(latent.shape, BF16),
        in_specs=[
            anywhere,
            anywhere,
            inside,
            inside,
            anywhere,
            anywhere,
            anywhere,
            anywhere,
            scalar,
            scalar,
            inside,
            anywhere,
            inside,
            inside,
            inside,
            inside,
        ],
        out_specs=inside,
        scratch_shapes=scratch,
        compiler_params=pltpu.CompilerParams(
            collective_id=0, has_side_effects=True, vmem_limit_bytes=60 * 1024 * 1024
        ),
        name="layer",
    )(
        latent,
        context,
        condition.reshape(WIDTH // 128, 128),
        context_condition.reshape(WIDTH // 128, 128),
        modulation,
        query_weight,
        key_weight,
        value_weight,
        lambdas,
        context_lift,
        head_gain.reshape(2, 128),
        output_weight,
        *tables,
    )


def solution(mesh):
    split = Mesh(mesh.devices.reshape(4, 4, 8, 2), ("y", "x", "z", "c"))
    plane = ("y", "x")
    column = ("z", "c")
    every = ("y", "x", "z", "c")
    return jax.shard_map(
        shards,
        mesh=split,
        in_specs=(
            P(every, None),
            P(plane, None),
            P(),
            P(),
            P(None, plane, column),
            P(None, column),
            P(None, column),
            P(None, column),
            P(column),
            P(column),
            P(),
            P(column, None),
        ),
        out_specs=P(every, None),
        check_vma=False,
    )
```

time: 306 us -> 102 us (0.33); the launches traced: 303 us -> 102 us
  waiting for transfers between devices: 157 us -> 0 us
  Pallas kernels: 0 us -> 99.1 us
  local copies, waits for them, and re-layouts: 39.2 us -> 1.67 us
  matrix products: 33.8 us -> 0 us
  starting transfers between devices: 19.7 us -> 0 us
  other arithmetic: 19.6 us -> 0 us
  blocking collectives: 18.6 us -> 0 us
  between operations: 14.6 us -> 1.3 us
    pallas_call x0 -> x1, Pallas kernels: none -> 99.1 us  [shards(): pl.pallas_call(body, out_shape=jax.ShapeDtypeStruct(latent.shape, BF16),...]
    all_gather x2 -> x0, waiting for transfers between devices: 75.1 us -> none  [the longest x1 41.4 us: shards(): segment = lax.all_gather(packed, SP, axis=0, tiled=True)]
    reduce_scatter x1 -> x0, waiting for transfers between devices: 60.2 us -> none  [shards(): lax.psum_scatter(jnp.dot(attended, output_weight, preferred_element_type=...]
    dot_general x22 -> x0, matrix products: 33.8 us -> none  [the longest x9 10.9 us: absorb(): jnp.einsum('mqhk,khd->mqhd', weights.astype(jnp.bfloat16), value_part, pr...]
    all_to_all x2 -> x0, waiting for transfers between devices: 21.5 us -> none  [from_everyone(): return lax.all_to_all(copies, axis, split_axis=0, concat_axis=0, tiled=True)]
    dynamic_slice x16 -> x0, local copies, waits for them, and re-layouts: 20.8 us -> none  [shards(): lax.scan(one_block, state_now, stacked)[0]]
    all_to_all x2 -> x0, starting transfers between devices: 19.4 us -> none  [from_everyone(): return lax.all_to_all(copies, axis, split_axis=0, concat_axis=0, tiled=True)]
    psum x2 -> x0, blocking collectives: 18.6 us -> none  [by_axis(): return functools.reduce(lax.psum, axes, shard)]
  transfers between devices with their start and end apart: 5 -> 0, of which waited for: 5 -> 0; matrix products, arithmetic and copies ran while one was open for 5% -> 0% of each run, Pallas kernels for 0% -> 0%
where the time goes in v1:
time: 102 us
  Pallas kernels  99.1 us (97%)
  local copies, waits for them, and re-layouts  1.67 us (2%)
  between operations  1.3 us (1%)
    pallas_call x1, Pallas kernels, shards(): pl.pallas_call(body, out_shape=jax.ShapeDtypeStruct(latent.shape, BF16),...  99.1 us

profile of v1, /device:TPU:1, one launch (start us, length us, event | category | flops | bytes accessed | tf_op | source)
XLA Modules:
  0.0 102.1 jit_solution(8165095105620191370)
XLA Ops:
  1.3 99.1 %layer.1 = bf16[32,4096]{1,0:T(8,128)(2,1)} custom-call(bf16[32,4096]{1,0:T(8,128)(2,1)} %latent.1, bf16[32,4096]{1,0:T(8,128)(2,1)} %context.1, f32[32,128]{1,0:T(8,128)} %bitcast.3, f32[32,128]{1,0:T(8,128)} %bitcast.4, bf16[3,256,256]{2,1,0:T(8,128)(2,1)} %modulation.1, bf16[4096,256]{1,0:T(8,128)(2,1)} %query_weight.1, bf16[4096,256]{1,0:T(8,128)(2,1)} %key_weight.1, ...), custom_call_target="tpu_custom_call" | custom-call | tf_op jit(solution)/shard_map/layer/pallas_call | solution.py:609
  100.5 1.7 %copy.20 = bf16[32,4096]{1,0:T(8,128)(2,1)} copy(bf16[32,4096]{1,0:T(8,128)(2,1)} %layer.1) | data formatting | bytes 524288

commit v2 on v1

v2 whole, which is shorter than its diff:
```python
import functools
import math

import jax
import jax.numpy as jnp
import numpy as np
from jax import lax
from jax.experimental import pallas as pl
from jax.experimental.pallas import tpu as pltpu
from jax.sharding import Mesh
from jax.sharding import PartitionSpec as P

MESH = pl.DeviceIdType.MESH
F32 = jnp.float32
BF16 = jnp.bfloat16

WIDTH = 4096
GRID_W = 64
ROPE_BASE = 10000.0
EPSILON = 1e-05
HEAD = 256
PART = 128
LOG2E = math.log2(math.e)
SCALE2 = PART ** (-0.5) * LOG2E
ROWS = 512
OWN = 32
CTX = 32
MEMBERS = 4
LAT_KEYS = MEMBERS * ROWS
KEYS = LAT_KEYS + MEMBERS * CTX
TILE = 256
OFFSET = (0, -1, 1, -2, 2, -3, 3, 4)
PASSES = ((0,), (1, 2), (3, 4), (5, 6), (7,))


def rope_tables():
    quarter = PART // 2
    eighth = PART // 4
    inverse = np.float32(ROPE_BASE) ** (-np.arange(eighth, dtype=np.float32) / np.float32(eighth))
    inverse = inverse.astype(np.float32)
    sign = np.concatenate([-np.ones(eighth), np.ones(eighth)]).astype(np.float32)

    def pair(count):
        angles = np.arange(count, dtype=np.float32)[:, None] * np.concatenate([inverse, inverse])
        angles = angles.astype(np.float32).astype(np.float64)
        return np.cos(angles).astype(np.float32), (np.sin(angles) * sign).astype(np.float32)

    row_cos, row_sin = pair(8192 // GRID_W)
    col_cos, col_sin = pair(GRID_W)
    none = np.zeros_like(row_cos)
    row_cos, row_sin = (np.concatenate([t, none], axis=1) for t in (row_cos, row_sin))
    none = np.zeros_like(col_cos)
    col_cos, col_sin = (np.concatenate([none, t], axis=1) for t in (col_cos, col_sin))
    half = GRID_W // 2
    both = [np.stack([t, np.concatenate([t[half:], t[:half]])]) for t in (col_cos, col_sin)]
    return row_cos, row_sin, both[0], both[1]


def body(
    latent,
    context,
    condition,
    context_condition,
    modulation,
    query_weight,
    key_weight,
    value_weight,
    lambdas,
    context_lift,
    head_gain,
    output_weight,
    row_cos,
    row_sin,
    col_cos,
    col_sin,
    result,
    res,
    lat,
    cond,
    cond_ctx,
    rows_cos,
    rows_sin,
    cols_cos,
    cols_sin,
    gx,
    ctx,
    modw,
    weights,
    xn,
    mod_in,
    mod_all,
    raw,
    qs,
    kv,
    outs,
    outs_in,
    tab,
    stats,
    stats_in,
    att,
    att_in,
    wout,
    part,
    sum_out,
    sum_in,
    load_sem,
    xs,
    xr,
    ps,
    pr,
    ms,
    mr,
    zs,
    zr,
    qsem_s,
    qsem_r,
    ksem_s,
    ksem_r,
    csem_s,
    csem_r,
    osem_s,
    osem_r,
    tsem_s,
    tsem_r,
    asem,
    wsem,
    rs,
    rr,
):
    y, x, z, c = (lax.axis_index(a) for a in ("y", "x", "z", "c"))
    sp = y * 4 + x
    waits = []

    def remote(src, dst, send, recv, to):
        return pltpu.make_async_remote_copy(
            src_ref=src, dst_ref=dst, send_sem=send, recv_sem=recv, device_id=to, device_id_type=MESH
        )

    def go(copy):
        copy.start()
        waits.append(copy)

    partner = {"c": 1 - c}

    def on_plane(dy, dx):
        return {"y": lax.rem(y + dy, 4), "x": lax.rem(x + dx, 4)}

    def on_z(d):
        return {"z": lax.rem(z + d + 8, 8)}

    def on_queries(d):
        return {"y": lax.rem(y + d * c, 4), "x": lax.rem(x + d * (1 - c), 4)}

    def on_keys(d):
        return {"y": lax.rem(y + d * (1 - c), 4), "x": lax.rem(x + d * c, 4)}

    pairs = (
        (latent, lat),
        (condition, cond),
        (context_condition, cond_ctx),
        (modulation, modw),
        (context, ctx),
        (row_cos, rows_cos),
        (row_sin, rows_sin),
        (col_cos, cols_cos),
        (col_sin, cols_sin),
        (query_weight, weights.at[0]),
        (key_weight, weights.at[1]),
        (value_weight, weights.at[2]),
        (output_weight, wout.at[0]),
    )
    loads = [pltpu.make_async_copy(a, b, load_sem.at[i]) for i, (a, b) in enumerate(pairs)]
    for load in loads:
        load.start()

    barrier = pltpu.get_barrier_semaphore()
    plane = [(dy, dx) for dy in range(4) for dx in range(4) if dy or dx]
    plane.sort(key=lambda d: -(min(d[0], 4 - d[0]) + min(d[1], 4 - d[1])))
    column = [(dz, dc) for dz in (4, 3, 5, 2, 6, 1, 7, 0) for dc in (1, 0) if dz or dc]

    def on_column(dz, dc):
        return {"z": lax.rem(z + dz, 8), "c": 1 - c if dc else c}

    peers = [on_column(*d) for d in column] + [on_plane(*d) for d in plane]
    for peer in peers:
        pl.semaphore_signal(barrier, inc=1, device_id=peer, device_id_type=MESH)

    def centered(src, g):
        v = src[pl.ds(pl.multiple_of(g * 16, 16), 16), :].astype(F32)
        v = v - jnp.mean(v, axis=-1, keepdims=True)
        spread = jnp.mean(jnp.square(v), axis=-1, keepdims=True)
        return v * lax.rsqrt(spread + EPSILON)

    def own_group(g, carry):
        gx[0, pl.ds(pl.multiple_of(g * 16, 16), 16), :] = centered(lat, g).astype(BF16)
        return carry

    loads[0].wait()
    lax.fori_loop(0, OWN // 16, own_group, 0)
    pl.semaphore_wait(barrier, len(peers))

    def ring_slot(way, k):
        return 0 if k == 0 else 7 if k == 4 else 2 * k - 1 if way == 0 else 2 * k

    def ring_copy(way, k, h):
        rows = pl.ds(16 * h, 16)
        return remote(
            gx.at[ring_slot(way, k - 1), rows],
            gx.at[ring_slot(way, k), rows],
            xs.at[way, k - 1, h],
            xr.at[way, k - 1, h],
            on_z(1 if way == 0 else -1),
        )

    def across(slot, h):
        return remote(
            gx.at[slot, pl.ds(16 * h, 16)],
            gx.at[slot, pl.ds(OWN + 16 * h, 16)],
            ps.at[slot, h],
            pr.at[slot, h],
            partner,
        )

    def relay(k, turn):
        for way in (0, 1):
            h = turn if way == 0 else 1 - turn
            if k == 4 and turn == 1:
                continue
            ring_copy(way, k, h).wait_recv()
            if k < 3 or (k == 3 and turn == 0):
                go(ring_copy(way, k + 1, h))
            go(across(ring_slot(way, k), h))

    for turn in (0, 1):
        for way in (0, 1):
            go(ring_copy(way, 1, turn if way == 0 else 1 - turn))
    for h in (0, 1):
        go(across(0, h))

    def silu_rows(ref):
        halves = [ref[pl.ds(2 * sp + i, 1), :] for i in (0, 1)]
        v = jnp.concatenate(halves, axis=1)
        return (v / (1.0 + jnp.exp(-v))).astype(BF16).astype(F32)

    for load in loads[1:4]:
        load.wait()
    own = silu_rows(cond)
    other = silu_rows(cond_ctx)
    at_row = lax.broadcasted_iota(jnp.int32, (16, 256), 0)
    partial = jnp.zeros((16, 256), F32)
    for r in range(3):
        lhs = jnp.where(at_row == 2 * r, own, jnp.where(at_row == 2 * r + 1, other, 0.0))
        partial += jnp.dot(lhs.astype(BF16), modw[r], preferred_element_type=F32)
    def tile_of(first):
        rows = partial[first : first + 4]
        return jnp.concatenate([rows[:, :PART], rows[:, PART:]], axis=0)

    mod_in[0, 0] = tile_of(0)
    mod_in[0, 1] = tile_of(4)

    def mod_copy(dy, dx):
        there = ((4 - dy) % 4) * 4 + (4 - dx) % 4
        return remote(
            mod_in.at[0], mod_in.at[there], ms.at[dy * 4 + dx], mr.at[there], on_plane(dy, dx)
        )

    for d in plane:
        go(mod_copy(*d))
    for d in plane:
        mod_copy(*d).wait_recv()

    def total_of(which):
        lines = [
            (mod_in[4 * i, which] + mod_in[4 * i + 1, which])
            + (mod_in[4 * i + 2, which] + mod_in[4 * i + 3, which])
            for i in range(4)
        ]
        return (lines[0] + lines[1]) + (lines[2] + lines[3])

    def spread(which):
        mod_all[which, z, c] = total_of(which)
        slab = mod_all.at[which, z, c]
        for dz, dc in column:
            there = ((8 - dz) % 8) * 2 + dc
            at = dz * 2 + dc
            go(remote(slab, slab, zs.at[which, at], zr.at[which, there], on_column(dz, dc)))

    def gathered(which):
        for dz, dc in column:
            slab = mod_all.at[which, lax.rem(z + dz, 8), 1 - c if dc else c]
            at = dz * 2 + dc
            remote(slab, slab, zs.at[which, at], zr.at[which, at], on_column(dz, dc)).wait_recv()

    spread(0)
    relay(1, 0)
    relay(1, 1)
    relay(2, 0)
    gathered(0)

    def shift_scale(t, which):
        tile = mod_all.at[0, t // 4, (t // 2) % 2]
        row = 4 * (t % 2) + which
        return tile[row : row + 1, :], 1.0 + tile[row + 2 : row + 3, :], slice(t * PART, (t + 1) * PART)

    def context_group(g, carry):
        v = centered(ctx, g)
        for t in range(32):
            offset, scaling, cols = shift_scale(t, 1)
            done = v[:, cols] * scaling + offset
            xn[pl.ds(pl.multiple_of(64 + g * 16, 16), 16), cols] = done.astype(BF16)
        return carry

    def modulated(slots):
        for t in range(32):
            offset, scaling, cols = shift_scale(t, 0)
            for i, slot in enumerate(slots):
                done = gx[slot, :, cols].astype(F32) * scaling + offset
                xn[64 * i : 64 * i + 64, cols] = done.astype(BF16)

    lane = lax.broadcasted_iota(jnp.int32, (64, PART), 1)
    low = lax.rem(lane, 64) < 32

    def project(count):
        def one(g, carry):
            raw[g, pl.ds(0, count)] = jnp.dot(
                xn[pl.ds(0, count), :], weights[g], preferred_element_type=F32
            ).astype(BF16)
            return carry

        lax.fori_loop(0, 3, one, 0)

    def step(p):
        slots = PASSES[p]
        modulated(slots)
        count = 64 * len(slots)
        if p == 0:
            loads[4].wait()
            lax.fori_loop(0, CTX // 16, context_group, 0)
            count += CTX
            for load in loads[5:12]:
                load.wait()
        project(count)
        for i, slot in enumerate(slots):
            line = sp * 8 + lax.rem(z + OFFSET[slot] + 8, 8)
            cosine = cols_cos[c] + rows_cos[pl.ds(line, 1), :]
            sine = cols_sin[c] + rows_sin[pl.ds(line, 1), :]
            base = 64 * slot
            for g in (0, 1):
                for m in (0, 1):
                    cols = slice(m * PART, (m + 1) * PART)
                    a = raw[g, 64 * i : 64 * i + 64, cols].astype(F32)
                    swapped = jnp.where(low, pltpu.roll(a, PART - 32, 1), pltpu.roll(a, 32, 1))
                    turned = (a * cosine + swapped * sine).astype(BF16)
                    if g == 0:
                        qs[0, base : base + 64, cols] = turned
                    else:
                        kv[base : base + 64, cols] = turned
            kv[base : base + 64, HEAD : 2 * HEAD] = raw[2, 64 * i : 64 * i + 64, :]
        if p == 0:
            kv[LAT_KEYS : LAT_KEYS + CTX, 0:HEAD] = raw[1, 64 : 64 + CTX, :]
            kv[LAT_KEYS : LAT_KEYS + CTX, HEAD : 2 * HEAD] = raw[2, 64 : 64 + CTX, :]
        for d in near(p):
            if p == 0:
                go(context_copy(d))
            go(key_copy(p, d))
        for d in near(p):
            go(query_copy(p, d))

    def near(p):
        return (2, 1, 3) if p == 4 else (1, 3)

    def rows_of(p):
        return 64 * PASSES[p][0], 64 * len(PASSES[p])

    def query_copy(p, d):
        start, count = rows_of(p)
        return remote(
            qs.at[0, pl.ds(start, count)],
            qs.at[4 - d, pl.ds(start, count)],
            qsem_s.at[p, d],
            qsem_r.at[p, 4 - d],
            on_queries(d),
        )

    def query_relay(p, d):
        start, count = rows_of(p)
        rows = pl.ds(start + (0 if d == 1 else count // 2), count // 2)
        at = 0 if d == 1 else 2
        return remote(
            qs.at[4 - d, rows], qs.at[2, rows], qsem_s.at[5 + p, at], qsem_r.at[5 + p, at], on_queries(d)
        )

    def key_copy(p, d):
        start, count = rows_of(p)
        return remote(
            kv.at[pl.ds(start, count)],
            kv.at[pl.ds((4 - d) * ROWS + start, count)],
            ksem_s.at[p, d],
            ksem_r.at[p, 4 - d],
            on_keys(d),
        )

    def key_relay(p, d):
        start, count = rows_of(p)
        start, count = start + (0 if d == 1 else count // 2), count // 2
        at = 0 if d == 1 else 2
        return remote(
            kv.at[pl.ds((4 - d) * ROWS + start, count)],
            kv.at[pl.ds(2 * ROWS + start, count)],
            ksem_s.at[5 + p, at],
            ksem_r.at[5 + p, at],
            on_keys(d),
        )

    def context_copy(d):
        return remote(
            kv.at[pl.ds(LAT_KEYS, CTX)],
            kv.at[pl.ds(LAT_KEYS + (4 - d) * CTX, CTX)],
            csem_s.at[d],
            csem_r.at[4 - d],
            on_keys(d),
        )

    def context_relay(d):
        at = 0 if d == 1 else 2
        skip = 0 if d == 1 else CTX // 2
        return remote(
            kv.at[pl.ds(LAT_KEYS + (4 - d) * CTX + skip, CTX // 2)],
            kv.at[pl.ds(LAT_KEYS + 2 * CTX + skip, CTX // 2)],
            csem_s.at[4 + at],
            csem_r.at[4 + at],
            on_keys(d),
        )

    def hand_on(p):
        for d in (1, 3):
            if p == 0:
                context_copy(d).wait_recv()
                go(context_relay(d))
            key_copy(p, d).wait_recv()
            go(key_relay(p, d))
        for d in (1, 3):
            query_copy(p, d).wait_recv()
            go(query_relay(p, d))

    def slots_in(slots, halves=(0, 1)):
        for slot in slots:
            for h in halves:
                across(slot, h).wait_recv()

    slots_in(PASSES[0])
    step(0)
    relay(2, 1)
    slots_in(PASSES[1])
    step(1)
    relay(3, 0)
    hand_on(0)
    slots_in(PASSES[2])
    step(2)
    relay(3, 1)
    hand_on(1)
    relay(4, 0)
    spread(1)
    slots_in(PASSES[3])
    step(3)
    hand_on(2)
    slots_in(PASSES[4])
    step(4)
    loads[12].wait()
    go(remote(wout.at[0], wout.at[1], wsem.at[0], wsem.at[1], partner))
    hand_on(3)

    for p in range(5):
        for copy in (query_copy, key_copy):
            if p == 4:
                for d in (1, 2, 3):
                    copy(p, d).wait_recv()
        for relayed in (query_relay, key_relay):
            if p < 4:
                for d in (1, 3):
                    relayed(p, d).wait_recv()
    for d in (1, 3):
        context_relay(d).wait_recv()

    lift = context_lift[0] * LOG2E
    column_of = lax.broadcasted_iota(jnp.int32, (TILE, PART), 1)

    def attend(p, parts=(0, 1)):
        first, count = rows_of(p)
        parts = [i for i in parts if i < count // 64]

        for i in parts:
            rows = pl.ds(first + 64 * i, 64)
            found = []
            for m in (0, 1):
                cols = slice(m * PART, (m + 1) * PART)
                q = qs[:, rows, cols].reshape(TILE, PART)
                s = lax.dot_general(
                    q, kv[:, cols], (((1,), (1,)), ((), ())), preferred_element_type=F32
                )
                near_s = s[:, :LAT_KEYS]
                far = s[:, LAT_KEYS:] * SCALE2 + lift
                peak = jnp.maximum(
                    jnp.max(near_s, axis=1, keepdims=True) * SCALE2,
                    jnp.max(far, axis=1, keepdims=True),
                )
                near_s = jnp.exp2(near_s * SCALE2 - peak)
                far = jnp.exp2(far - peak)
                total = jnp.sum(near_s, axis=1, keepdims=True) + jnp.sum(far, axis=1, keepdims=True)
                o = jnp.dot(
                    near_s.astype(BF16), kv[:LAT_KEYS, HEAD : 2 * HEAD], preferred_element_type=F32
                ) + jnp.dot(
                    far.astype(BF16), kv[LAT_KEYS:, HEAD : 2 * HEAD], preferred_element_type=F32
                )
                o = (o / total).astype(BF16).reshape(MEMBERS, 64, HEAD)
                outs[:, rows, m * HEAD : (m + 1) * HEAD] = o
                found += [peak, total]
            table = jnp.where(
                column_of == 0,
                found[0],
                jnp.where(column_of == 1, found[1], jnp.where(column_of == 2, found[2], found[3])),
            )
            tab[i] = table.reshape(MEMBERS, 64, PART)
        if parts[-1] < count // 64 - 1:
            return
        for j in range(MEMBERS):
            second = tab[1, j] if count > 64 else jnp.zeros((64, PART), F32)
            stats[p, j] = jnp.concatenate([tab[0, j], second], axis=0).T[:8, :]
        for j in (2, 1, 3):
            for copy in out_copies(p, j):
                go(copy)

    def out_copies(p, j):
        start, count = rows_of(p)
        rows = pl.ds(start, count)
        to = on_queries(j)
        return (
            remote(
                outs.at[j, rows],
                outs_in.at[4 - j, rows],
                osem_s.at[p, j],
                osem_r.at[p, 4 - j],
                to,
            ),
            remote(
                stats.at[p, j],
                stats_in.at[p, 4 - j],
                tsem_s.at[p, j],
                tsem_r.at[p, 4 - j],
                to,
            ),
        )

    def swap(p):
        slots = pl.ds(PASSES[p][0], len(PASSES[p]))
        return remote(
            att.at[slots, 1], att_in.at[slots], asem.at[0, p], asem.at[1, p], partner
        )

    def combine(p):
        for j in (3, 1, 2):
            for copy in out_copies(p, j):
                copy.wait_recv()
        start, count = rows_of(p)
        rows = slice(start, start + count)
        tables = [stats[p, 0]] + [stats_in[p, j] for j in (1, 2, 3)]
        turned = jnp.concatenate(tables + [jnp.zeros((96, PART), F32)], axis=0).T[:count]
        means = []
        for m in (0, 1):
            peaks = [turned[:, 8 * j + 2 * m : 8 * j + 2 * m + 1] for j in range(4)]
            totals = [turned[:, 8 * j + 2 * m + 1 : 8 * j + 2 * m + 2] for j in range(4)]
            top = jnp.maximum(jnp.maximum(peaks[0], peaks[1]), jnp.maximum(peaks[2], peaks[3]))
            shares = [t * jnp.exp2(k - top) for k, t in zip(peaks, totals)]
            whole = (shares[0] + shares[1]) + (shares[2] + shares[3])
            cols = slice(m * HEAD, (m + 1) * HEAD)
            acc = outs[0, rows, cols].astype(F32) * (shares[0] / whole)
            for j in (1, 2, 3):
                acc += outs_in[j, rows, cols].astype(F32) * (shares[j] / whole)
            means.append(acc)
        difference = means[0] - lambdas[0] * means[1]
        spread = jnp.mean(jnp.square(difference), axis=1, keepdims=True)
        gain = jnp.concatenate([head_gain[0:1, :], head_gain[1:2, :]], axis=1)
        scaled = difference * lax.rsqrt(spread + EPSILON) * gain
        slot, many = PASSES[p][0], len(PASSES[p])
        att[slot : slot + many] = scaled.astype(BF16).reshape(many, 2, OWN, HEAD)
        go(swap(p))

    def multiply(p):
        swap(p).wait_recv()
        slot, many = PASSES[p][0], len(PASSES[p])
        mine = att[slot : slot + many, 0].reshape(many * OWN, HEAD)
        theirs = att_in[slot : slot + many].reshape(many * OWN, HEAD)
        for n in range(2):
            cols = slice(n * 2048, (n + 1) * 2048)
            got = jnp.dot(mine, wout[0, :, cols], preferred_element_type=F32)
            got += jnp.dot(theirs, wout[1, :, cols], preferred_element_type=F32)
            part[slot : slot + many, :, cols] = got.reshape(many, OWN, 2048)

    def sum_slot(way, t):
        return 7 if t == 1 else 2 * (5 - t) if way == 0 else 2 * (5 - t) - 1

    def sum_copy(way, t, h):
        return remote(
            sum_out.at[way, t - 1, h],
            sum_in.at[way, t - 1, h],
            rs.at[way, t - 1, h],
            rr.at[way, t - 1, h],
            on_z(1 if way == 0 else -1),
        )

    def send_sum(way, t, h, add):
        slot = sum_slot(way, t)
        for n in range(4):
            cols = slice(n * 1024, (n + 1) * 1024)
            total = part[slot, 16 * h : 16 * h + 16, cols]
            if add:
                total = total + sum_in[way, t - 2, h, :, cols].astype(F32)
            sum_out[way, t - 1, h, :, cols] = total.astype(BF16)
        go(sum_copy(way, t, h))

    def add_on(t, turns):
        for turn in turns:
            for way in (0, 1):
                h = turn if way == 0 else 1 - turn
                sum_copy(way, t - 1, h).wait_recv()
                send_sum(way, t, h, True)

    attend(4)
    attend(3)
    combine(4)
    attend(2, (0,))
    remote(wout.at[0], wout.at[1], wsem.at[0], wsem.at[1], partner).wait_recv()
    multiply(4)
    for way in (0, 1):
        send_sum(way, 1, way, False)
    attend(2, (1,))
    combine(3)
    attend(1, (0,))
    multiply(3)
    for way in (0, 1):
        send_sum(way, 2, 1 - way, False)
    add_on(2, (0,))
    attend(1, (1,))
    combine(2)
    attend(0)
    multiply(2)
    add_on(3, (1, 0))
    combine(1)
    combine(0)
    multiply(1)
    add_on(4, (1, 0))
    multiply(0)
    gathered(1)
    for turn in (1, 0):
        for way in (0, 1):
            sum_copy(way, 4, turn if way == 0 else 1 - turn).wait_recv()
    for h in (0, 1):
        rows = slice(16 * h, 16 * h + 16)
        for t in range(32):
            cols = slice(t * PART, (t + 1) * PART)
            mixture = part[0, rows, cols] + (
                sum_in[0, 3, h, :, cols].astype(F32) + sum_in[1, 3, h, :, cols].astype(F32)
            )
            row = 4 * (t % 2)
            gate = mod_all[1, t // 4, (t // 2) % 2, row : row + 1, :]
            res[rows, cols] = (lat[rows, cols].astype(F32) + gate * mixture).astype(BF16)

    store = pltpu.make_async_copy(res, result, load_sem.at[13])
    store.start()
    for copy in waits:
        copy.wait_send()
    store.wait()


def shards(*args):
    (
        latent,
        context,
        condition,
        context_condition,
        modulation,
        query_weight,
        key_weight,
        value_weight,
        lambdas,
        context_lift,
        head_gain,
        output_weight,
    ) = args
    anywhere = pl.BlockSpec(memory_space=pl.ANY)
    inside = pl.BlockSpec(memory_space=pltpu.VMEM)
    scalar = pl.BlockSpec(memory_space=pltpu.SMEM)
    tables = rope_tables()
    dma = pltpu.SemaphoreType.DMA
    scratch = [
        pltpu.VMEM((OWN, WIDTH), BF16),
        pltpu.VMEM((OWN, WIDTH), BF16),
        pltpu.VMEM((WIDTH // 128, 128), F32),
        pltpu.VMEM((WIDTH // 128, 128), F32),
        pltpu.VMEM((8192 // GRID_W, PART), F32),
        pltpu.VMEM((8192 // GRID_W, PART), F32),
        pltpu.VMEM((2, GRID_W, PART), F32),
        pltpu.VMEM((2, GRID_W, PART), F32),
        pltpu.VMEM((8, 64, WIDTH), BF16),
        pltpu.VMEM((CTX, WIDTH), BF16),
        pltpu.VMEM((3, 256, 256), BF16),
        pltpu.VMEM((3, WIDTH, HEAD), BF16),
        pltpu.VMEM((128, WIDTH), BF16),
        pltpu.VMEM((16, 2, 8, PART), F32),
        pltpu.VMEM((2, 8, 2, 8, PART), F32),
        pltpu.VMEM((3, 128, HEAD), BF16),
        pltpu.VMEM((4, ROWS, HEAD), BF16),
        pltpu.VMEM((KEYS, 2 * HEAD), BF16),
        pltpu.VMEM((4, ROWS, 2 * HEAD), BF16),
        pltpu.VMEM((4, ROWS, 2 * HEAD), BF16),
        pltpu.VMEM((2, MEMBERS, 64, PART), F32),
        pltpu.VMEM((5, MEMBERS, 8, PART), F32),
        pltpu.VMEM((5, MEMBERS, 8, PART), F32),
        pltpu.VMEM((8, 2, OWN, HEAD), BF16),
        pltpu.VMEM((8, OWN, HEAD), BF16),
        pltpu.VMEM((2, HEAD, WIDTH), BF16),
        pltpu.VMEM((8, OWN, WIDTH), F32),
        pltpu.VMEM((2, 4, 2, 16, WIDTH), BF16),
        pltpu.VMEM((2, 4, 2, 16, WIDTH), BF16),
        dma((14,)),
        dma((2, 4, 2)),
        dma((2, 4, 2)),
        dma((8, 2)),
        dma((8, 2)),
        dma((16,)),
        dma((16,)),
        dma((2, 16)),
        dma((2, 16)),
        dma((10, 4)),
        dma((10, 4)),
        dma((10, 4)),
        dma((10, 4)),
        dma((8,)),
        dma((8,)),
        dma((5, 4)),
        dma((5, 4)),
        dma((5, 4)),
        dma((5, 4)),
        dma((2, 5)),
        dma((2,)),
        dma((2, 4, 2)),
        dma((2, 4, 2)),
    ]
    return pl.pallas_call(
        body,
        out_shape=jax.ShapeDtypeStruct(latent.shape, BF16),
        in_specs=[anywhere] * 8 + [scalar, scalar, inside] + [anywhere] * 5,
        out_specs=anywhere,
        scratch_shapes=scratch,
        compiler_params=pltpu.CompilerParams(
            collective_id=0, has_side_effects=True, vmem_limit_bytes=60 * 1024 * 1024
        ),
        name="layer",
    )(
        latent,
        context,
        condition.reshape(WIDTH // 128, 128),
        context_condition.reshape(WIDTH // 128, 128),
        modulation,
        query_weight,
        key_weight,
        value_weight,
        lambdas,
        context_lift,
        head_gain.reshape(2, 128),
        output_weight,
        *tables,
    )


def solution(mesh):
    split = Mesh(mesh.devices.reshape(4, 4, 8, 2), ("y", "x", "z", "c"))
    plane = ("y", "x")
    column = ("z", "c")
    every = ("y", "x", "z", "c")
    return jax.shard_map(
        shards,
        mesh=split,
        in_specs=(
            P(every, None),
            P(plane, None),
            P(),
            P(),
            P(None, plane, column),
            P(None, column),
            P(None, column),
            P(None, column),
            P(column),
            P(column),
            P(),
            P(column, None),
        ),
        out_specs=P(every, None),
        check_vma=False,
    )
```

time: 102 us -> 89.5 us (0.88)
  Pallas kernels: 99.1 us -> 86.4 us
    pallas_call x1, Pallas kernels: 99.1 us -> 86.4 us  [shards(): pl.pallas_call(body, out_shape=jax.ShapeDtypeStruct(latent.shape, BF16),...]
where the time goes in v2:
time: 89.5 us; the launch traced here: 89.3 us
  Pallas kernels  86.4 us (97%)
  local copies, waits for them, and re-layouts  1.67 us (2%)
  between operations  1.31 us (1%)
    pallas_call x1, Pallas kernels, shards(): pl.pallas_call(body, out_shape=jax.ShapeDtypeStruct(latent.shape, BF16),...  86.4 us

profile of v2, /device:TPU:1, one launch (start us, length us, event | category | flops | bytes accessed | tf_op | source)
XLA Modules:
  0.0 89.3 jit_solution(3005443729380250594)
XLA Ops:
  1.3 86.4 %layer.1 = bf16[32,4096]{1,0:T(8,128)(2,1)} custom-call(bf16[32,4096]{1,0:T(8,128)(2,1)} %latent.1, bf16[32,4096]{1,0:T(8,128)(2,1)} %context.1, f32[32,128]{1,0:T(8,128)} %bitcast.3, f32[32,128]{1,0:T(8,128)} %bitcast.4, bf16[3,256,256]{2,1,0:T(8,128)(2,1)} %modulation.1, bf16[4096,256]{1,0:T(8,128)(2,1)} %query_weight.1, bf16[4096,256]{1,0:T(8,128)(2,1)} %key_weight.1, ...), custom_call_target="tpu_custom_call" | custom-call | tf_op jit(solution)/shard_map/layer/pallas_call | solution.py:749
  87.7 1.7 %copy.20 = bf16[32,4096]{1,0:T(8,128)(2,1)} copy(bf16[32,4096]{1,0:T(8,128)(2,1)} %layer.1) | data formatting | bytes 524288

commit v3 on v2

--- a/solution.py
+++ b/solution.py
@@ -104,33 +104,20 @@
     sum_out,
     sum_in,
     load_sem,
-    xs,
+    sent,
     xr,
-    ps,
     pr,
-    ms,
     mr,
-    zs,
-    zr,
-    qsem_s,
-    qsem_r,
-    ksem_s,
-    ksem_r,
-    csem_s,
-    csem_r,
-    osem_s,
-    osem_r,
-    tsem_s,
-    tsem_r,
-    asem,
-    wsem,
-    rs,
+    qr,
+    kr,
+    outs_r,
+    stats_r,
+    att_r,
+    wout_r,
     rr,
 ):
     y, x, z, c = (lax.axis_index(a) for a in ("y", "x", "z", "c"))
     sp = y * 4 + x
-    waits = []
-
     def remote(src, dst, send, recv, to):
         return pltpu.make_async_remote_copy(
             src_ref=src, dst_ref=dst, send_sem=send, recv_sem=recv, device_id=to, device_id_type=MESH
@@ -138,7 +125,9 @@
 
     def go(copy):
         copy.start()
-        waits.append(copy)
+
+    def arrived(ref, semaphore):
+        pltpu.make_async_copy(ref, ref, semaphore).wait()
 
     partner = {"c": 1 - c}
 
@@ -207,8 +196,8 @@
         return remote(
             gx.at[ring_slot(way, k - 1), rows],
             gx.at[ring_slot(way, k), rows],
-            xs.at[way, k - 1, h],
-            xr.at[way, k - 1, h],
+            sent.at[0],
+            xr.at[way, 2 * (k - 1) + (h if k < 4 else 0)],
             on_z(1 if way == 0 else -1),
         )
 
@@ -216,8 +205,8 @@
         return remote(
             gx.at[slot, pl.ds(16 * h, 16)],
             gx.at[slot, pl.ds(OWN + 16 * h, 16)],
-            ps.at[slot, h],
-            pr.at[slot, h],
+            sent.at[1],
+            pr.at[slot],
             partner,
         )
 
@@ -261,13 +250,12 @@
     def mod_copy(dy, dx):
         there = ((4 - dy) % 4) * 4 + (4 - dx) % 4
         return remote(
-            mod_in.at[0], mod_in.at[there], ms.at[dy * 4 + dx], mr.at[there], on_plane(dy, dx)
+            mod_in.at[0], mod_in.at[there], sent.at[2], mr.at[0], on_plane(dy, dx)
         )
 
     for d in plane:
         go(mod_copy(*d))
-    for d in plane:
-        mod_copy(*d).wait_recv()
+    arrived(mod_in.at[pl.ds(1, 15)], mr.at[0])
 
     def total_of(which):
         lines = [
@@ -278,18 +266,13 @@
         return (lines[0] + lines[1]) + (lines[2] + lines[3])
 
     def spread(which):
-        mod_all[which, z, c] = total_of(which)
-        slab = mod_all.at[which, z, c]
-        for dz, dc in column:
-            there = ((8 - dz) % 8) * 2 + dc
-            at = dz * 2 + dc
-            go(remote(slab, slab, zs.at[which, at], zr.at[which, there], on_column(dz, dc)))
+        mod_all[which, 2 * z + c] = total_of(which)
+        slab = mod_all.at[which, 2 * z + c]
+        for d in column:
+            go(remote(slab, slab, sent.at[3 + which], mr.at[1 + which], on_column(*d)))
 
     def gathered(which):
-        for dz, dc in column:
-            slab = mod_all.at[which, lax.rem(z + dz, 8), 1 - c if dc else c]
-            at = dz * 2 + dc
-            remote(slab, slab, zs.at[which, at], zr.at[which, at], on_column(dz, dc)).wait_recv()
+        arrived(mod_all.at[which, pl.ds(0, 15)], mr.at[1 + which])
 
     spread(0)
     relay(1, 0)
@@ -298,7 +281,7 @@
     gathered(0)
 
     def shift_scale(t, which):
-        tile = mod_all.at[0, t // 4, (t // 2) % 2]
+        tile = mod_all.at[0, t // 2]
         row = 4 * (t % 2) + which
         return tile[row : row + 1, :], 1.0 + tile[row + 2 : row + 3, :], slice(t * PART, (t + 1) * PART)
 
@@ -320,32 +303,33 @@
     lane = lax.broadcasted_iota(jnp.int32, (64, PART), 1)
     low = lax.rem(lane, 64) < 32
 
-    def project(count):
+    def project(count, first, last):
         def one(g, carry):
             raw[g, pl.ds(0, count)] = jnp.dot(
                 xn[pl.ds(0, count), :], weights[g], preferred_element_type=F32
             ).astype(BF16)
             return carry
 
-        lax.fori_loop(0, 3, one, 0)
+        lax.fori_loop(first, last, one, 0)
 
     def step(p):
         slots = PASSES[p]
         modulated(slots)
         count = 64 * len(slots)
+        latent_count = count
         if p == 0:
             loads[4].wait()
             lax.fori_loop(0, CTX // 16, context_group, 0)
             count += CTX
             for load in loads[5:12]:
                 load.wait()
-        project(count)
-        for i, slot in enumerate(slots):
-            line = sp * 8 + lax.rem(z + OFFSET[slot] + 8, 8)
-            cosine = cols_cos[c] + rows_cos[pl.ds(line, 1), :]
-            sine = cols_sin[c] + rows_sin[pl.ds(line, 1), :]
-            base = 64 * slot
-            for g in (0, 1):
+
+        def turn(g):
+            for i, slot in enumerate(slots):
+                line = sp * 8 + lax.rem(z + OFFSET[slot] + 8, 8)
+                cosine = cols_cos[c] + rows_cos[pl.ds(line, 1), :]
+                sine = cols_sin[c] + rows_sin[pl.ds(line, 1), :]
+                base = 64 * slot
                 for m in (0, 1):
                     cols = slice(m * PART, (m + 1) * PART)
                     a = raw[g, 64 * i : 64 * i + 64, cols].astype(F32)
@@ -355,7 +339,11 @@
                         qs[0, base : base + 64, cols] = turned
                     else:
                         kv[base : base + 64, cols] = turned
-            kv[base : base + 64, HEAD : 2 * HEAD] = raw[2, 64 * i : 64 * i + 64, :]
+
+        project(count, 1, 3)
+        turn(1)
+        base = 64 * slots[0]
+        kv[base : base + latent_count, HEAD : 2 * HEAD] = raw[2, :latent_count, :]
         if p == 0:
             kv[LAT_KEYS : LAT_KEYS + CTX, 0:HEAD] = raw[1, 64 : 64 + CTX, :]
             kv[LAT_KEYS : LAT_KEYS + CTX, HEAD : 2 * HEAD] = raw[2, 64 : 64 + CTX, :]
@@ -363,6 +351,8 @@
             if p == 0:
                 go(context_copy(d))
             go(key_copy(p, d))
+        project(latent_count, 0, 1)
+        turn(0)
         for d in near(p):
             go(query_copy(p, d))
 
@@ -377,17 +367,16 @@
         return remote(
             qs.at[0, pl.ds(start, count)],
             qs.at[4 - d, pl.ds(start, count)],
-            qsem_s.at[p, d],
-            qsem_r.at[p, 4 - d],
+            sent.at[5],
+            qr.at[p],
             on_queries(d),
         )
 
     def query_relay(p, d):
         start, count = rows_of(p)
         rows = pl.ds(start + (0 if d == 1 else count // 2), count // 2)
-        at = 0 if d == 1 else 2
-        return remote(
-            qs.at[4 - d, rows], qs.at[2, rows], qsem_s.at[5 + p, at], qsem_r.at[5 + p, at], on_queries(d)
+        return remote(
+            qs.at[4 - d, rows], qs.at[2, rows], sent.at[5], qr.at[5 + p], on_queries(d)
         )
 
     def key_copy(p, d):
@@ -395,20 +384,19 @@
         return remote(
             kv.at[pl.ds(start, count)],
             kv.at[pl.ds((4 - d) * ROWS + start, count)],
-            ksem_s.at[p, d],
-            ksem_r.at[p, 4 - d],
+            sent.at[6],
+            kr.at[p],
             on_keys(d),
         )
 
     def key_relay(p, d):
         start, count = rows_of(p)
         start, count = start + (0 if d == 1 else count // 2), count // 2
-        at = 0 if d == 1 else 2
         return remote(
             kv.at[pl.ds((4 - d) * ROWS + start, count)],
             kv.at[pl.ds(2 * ROWS + start, count)],
-            ksem_s.at[5 + p, at],
-            ksem_r.at[5 + p, at],
+            sent.at[6],
+            kr.at[5 + p],
             on_keys(d),
         )
 
@@ -416,37 +404,37 @@
         return remote(
             kv.at[pl.ds(LAT_KEYS, CTX)],
             kv.at[pl.ds(LAT_KEYS + (4 - d) * CTX, CTX)],
-            csem_s.at[d],
-            csem_r.at[4 - d],
+            sent.at[6],
+            kr.at[0],
             on_keys(d),
         )
 
     def context_relay(d):
-        at = 0 if d == 1 else 2
         skip = 0 if d == 1 else CTX // 2
         return remote(
             kv.at[pl.ds(LAT_KEYS + (4 - d) * CTX + skip, CTX // 2)],
             kv.at[pl.ds(LAT_KEYS + 2 * CTX + skip, CTX // 2)],
-            csem_s.at[4 + at],
-            csem_r.at[4 + at],
+            sent.at[6],
+            kr.at[5],
             on_keys(d),
         )
 
+    def rows_in(p, share):
+        return rows_of(p)[1] * share + (CTX * share if p == 0 else 0)
+
     def hand_on(p):
+        arrived(kv.at[pl.ds(0, rows_in(p, 2))], kr.at[p])
         for d in (1, 3):
             if p == 0:
-                context_copy(d).wait_recv()
                 go(context_relay(d))
-            key_copy(p, d).wait_recv()
             go(key_relay(p, d))
+        arrived(qs.at[pl.ds(0, 2), pl.ds(0, rows_of(p)[1])], qr.at[p])
         for d in (1, 3):
-            query_copy(p, d).wait_recv()
             go(query_relay(p, d))
 
-    def slots_in(slots, halves=(0, 1)):
+    def slots_in(slots):
         for slot in slots:
-            for h in halves:
-                across(slot, h).wait_recv()
+            arrived(gx.at[slot, pl.ds(0, OWN)], pr.at[slot])
 
     slots_in(PASSES[0])
     step(0)
@@ -459,28 +447,22 @@
     step(2)
     relay(3, 1)
     hand_on(1)
-    relay(4, 0)
-    spread(1)
     slots_in(PASSES[3])
     step(3)
+    relay(4, 0)
     hand_on(2)
     slots_in(PASSES[4])
     step(4)
+    spread(1)
     loads[12].wait()
-    go(remote(wout.at[0], wout.at[1], wsem.at[0], wsem.at[1], partner))
+    go(remote(wout.at[0], wout.at[1], sent.at[11], wout_r, partner))
     hand_on(3)
 
-    for p in range(5):
-        for copy in (query_copy, key_copy):
-            if p == 4:
-                for d in (1, 2, 3):
-                    copy(p, d).wait_recv()
-        for relayed in (query_relay, key_relay):
-            if p < 4:
-                for d in (1, 3):
-                    relayed(p, d).wait_recv()
-    for d in (1, 3):
-        context_relay(d).wait_recv()
+    for p in range(4):
+        arrived(kv.at[pl.ds(0, rows_in(p, 1))], kr.at[5 + p])
+        arrived(qs.at[0, pl.ds(0, rows_of(p)[1])], qr.at[5 + p])
+    arrived(kv.at[pl.ds(0, rows_in(4, 3))], kr.at[4])
+    arrived(qs.at[pl.ds(0, 3), pl.ds(0, rows_of(4)[1])], qr.at[4])
 
     lift = context_lift[0] * LOG2E
     column_of = lax.broadcasted_iota(jnp.int32, (TILE, PART), 1)
@@ -538,15 +520,15 @@
             remote(
                 outs.at[j, rows],
                 outs_in.at[4 - j, rows],
-                osem_s.at[p, j],
-                osem_r.at[p, 4 - j],
+                sent.at[7],
+                outs_r.at[p],
                 to,
             ),
             remote(
                 stats.at[p, j],
                 stats_in.at[p, 4 - j],
-                tsem_s.at[p, j],
-                tsem_r.at[p, 4 - j],
+                sent.at[8],
+                stats_r.at[p],
                 to,
             ),
         )
@@ -554,14 +536,13 @@
     def swap(p):
         slots = pl.ds(PASSES[p][0], len(PASSES[p]))
         return remote(
-            att.at[slots, 1], att_in.at[slots], asem.at[0, p], asem.at[1, p], partner
+            att.at[slots, 1], att_in.at[slots], sent.at[9], att_r.at[p], partner
         )
 
     def combine(p):
-        for j in (3, 1, 2):
-            for copy in out_copies(p, j):
-                copy.wait_recv()
         start, count = rows_of(p)
+        arrived(outs_in.at[pl.ds(1, 3), pl.ds(start, count)], outs_r.at[p])
+        arrived(stats_in.at[p, pl.ds(1, 3)], stats_r.at[p])
         rows = slice(start, start + count)
         tables = [stats[p, 0]] + [stats_in[p, j] for j in (1, 2, 3)]
         turned = jnp.concatenate(tables + [jnp.zeros((96, PART), F32)], axis=0).T[:count]
@@ -603,8 +584,8 @@
         return remote(
             sum_out.at[way, t - 1, h],
             sum_in.at[way, t - 1, h],
-            rs.at[way, t - 1, h],
-            rr.at[way, t - 1, h],
+            sent.at[10],
+            rr.at[way, 0 if t == 1 else 2 * t - 3 + h],
             on_z(1 if way == 0 else -1),
         )
 
@@ -629,7 +610,7 @@
     attend(3)
     combine(4)
     attend(2, (0,))
-    remote(wout.at[0], wout.at[1], wsem.at[0], wsem.at[1], partner).wait_recv()
+    remote(wout.at[0], wout.at[1], sent.at[11], wout_r, partner).wait_recv()
     multiply(4)
     for way in (0, 1):
         send_sum(way, 1, way, False)
@@ -662,13 +643,29 @@
                 sum_in[0, 3, h, :, cols].astype(F32) + sum_in[1, 3, h, :, cols].astype(F32)
             )
             row = 4 * (t % 2)
-            gate = mod_all[1, t // 4, (t // 2) % 2, row : row + 1, :]
+            gate = mod_all[1, t // 2, row : row + 1, :]
             res[rows, cols] = (lat[rows, cols].astype(F32) + gate * mixture).astype(BF16)
 
     store = pltpu.make_async_copy(res, result, load_sem.at[13])
     store.start()
-    for copy in waits:
-        copy.wait_send()
+    ring_bytes = gx.at[pl.ds(0, 7), pl.ds(0, OWN)]
+    for i, ref in enumerate(
+        (
+            ring_bytes,
+            gx.at[:, pl.ds(0, OWN)],
+            mod_in.at[pl.ds(1, 15)],
+            mod_all.at[0, pl.ds(0, 15)],
+            mod_all.at[1, pl.ds(0, 15)],
+            qs.at[pl.ds(0, 3)],
+            kv.at[pl.ds(0, 3 * (ROWS + CTX))],
+            outs.at[pl.ds(1, 3)],
+            stats.at[:, pl.ds(1, 3)],
+            att.at[:, 1],
+            ring_bytes,
+            wout.at[0],
+        )
+    ):
+        arrived(ref, sent.at[i])
     store.wait()
 
 
@@ -707,7 +704,7 @@
         pltpu.VMEM((3, WIDTH, HEAD), BF16),
         pltpu.VMEM((128, WIDTH), BF16),
         pltpu.VMEM((16, 2, 8, PART), F32),
-        pltpu.VMEM((2, 8, 2, 8, PART), F32),
+        pltpu.VMEM((2, 16, 8, PART), F32),
         pltpu.VMEM((3, 128, HEAD), BF16),
         pltpu.VMEM((4, ROWS, HEAD), BF16),
         pltpu.VMEM((KEYS, 2 * HEAD), BF16),
@@ -723,28 +720,17 @@
         pltpu.VMEM((2, 4, 2, 16, WIDTH), BF16),
         pltpu.VMEM((2, 4, 2, 16, WIDTH), BF16),
         dma((14,)),
-        dma((2, 4, 2)),
-        dma((2, 4, 2)),
-        dma((8, 2)),
-        dma((8, 2)),
-        dma((16,)),
-        dma((16,)),
-        dma((2, 16)),
-        dma((2, 16)),
-        dma((10, 4)),
-        dma((10, 4)),
-        dma((10, 4)),
-        dma((10, 4)),
+        dma((12,)),
+        dma((2, 7)),
         dma((8,)),
-        dma((8,)),
-        dma((5, 4)),
-        dma((5, 4)),
-        dma((5, 4)),
-        dma((5, 4)),
-        dma((2, 5)),
-        dma((2,)),
-        dma((2, 4, 2)),
-        dma((2, 4, 2)),
+        dma((3,)),
+        dma((9,)),
+        dma((9,)),
+        dma((5,)),
+        dma((5,)),
+        dma((5,)),
+        dma(()),
+        dma((2, 7)),
     ]
     return pl.pallas_call(
         body,

time: 89.5 us -> 85 us (0.950)
  Pallas kernels: 86.4 us -> 81.9 us
    pallas_call x1, Pallas kernels: 86.4 us -> 81.9 us  [shards(): pl.pallas_call(body, out_shape=jax.ShapeDtypeStruct(latent.shape, BF16),...]
where the time goes in v3:
time: 85 us; the launch traced here: 84.9 us
  Pallas kernels  81.9 us (96%)
  local copies, waits for them, and re-layouts  1.67 us (2%)
  between operations  1.31 us (2%)
    pallas_call x1, Pallas kernels, shards(): pl.pallas_call(body, out_shape=jax.ShapeDtypeStruct(latent.shape, BF16),...  81.9 us

profile of v3, /device:TPU:1, one launch (start us, length us, event | category | flops | bytes accessed | tf_op | source)
XLA Modules:
  0.0 84.9 jit_solution(8049769595950843875)
XLA Ops:
  1.3 81.9 %layer.1 = bf16[32,4096]{1,0:T(8,128)(2,1)} custom-call(bf16[32,4096]{1,0:T(8,128)(2,1)} %latent.1, bf16[32,4096]{1,0:T(8,128)(2,1)} %context.1, f32[32,128]{1,0:T(8,128)} %bitcast.3, f32[32,128]{1,0:T(8,128)} %bitcast.4, bf16[3,256,256]{2,1,0:T(8,128)(2,1)} %modulation.1, bf16[4096,256]{1,0:T(8,128)(2,1)} %query_weight.1, bf16[4096,256]{1,0:T(8,128)(2,1)} %key_weight.1, ...), custom_call_target="tpu_custom_call" | custom-call | tf_op jit(solution)/shard_map/layer/pallas_call | solution.py:735
  83.2 1.7 %copy.20 = bf16[32,4096]{1,0:T(8,128)(2,1)} copy(bf16[32,4096]{1,0:T(8,128)(2,1)} %layer.1) | data formatting | bytes 524288

commit v4 on v3

--- a/solution.py
+++ b/solution.py
@@ -94,6 +94,8 @@
     kv,
     outs,
     outs_in,
+    score_buf,
+    peak_buf,
     tab,
     stats,
     stats_in,
@@ -467,70 +469,82 @@
     lift = context_lift[0] * LOG2E
     column_of = lax.broadcasted_iota(jnp.int32, (TILE, PART), 1)
 
+    def beside(scored, weighed):
+        q = total = o = top = None
+        if scored:
+            slot, m = scored
+            cols = slice(m * PART, (m + 1) * PART)
+            q = qs[:, 64 * slot : 64 * slot + 64, cols].reshape(TILE, PART)
+        if weighed:
+            peak = jnp.max(peak_buf[weighed[1]], axis=1, keepdims=True)
+            total = jnp.zeros((TILE, PART), F32)
+            o = jnp.zeros((TILE, HEAD), F32)
+        for first in range(0, KEYS, 256):
+            last = min(first + 256, KEYS)
+            lanes = range((last - first) // PART)
+            if weighed:
+                w = jnp.exp2(score_buf[weighed[1], :, first:last] - peak)
+                for i in lanes:
+                    total += w[:, i * PART : (i + 1) * PART]
+            if scored:
+                t = lax.dot_general(
+                    q, kv[first:last, cols], (((1,), (1,)), ((), ())), preferred_element_type=F32
+                )
+                t = t * SCALE2
+                if first >= LAT_KEYS:
+                    t = t + lift
+                score_buf[m, :, first:last] = t
+                for i in lanes:
+                    part_t = t[:, i * PART : (i + 1) * PART]
+                    top = part_t if top is None else jnp.maximum(top, part_t)
+            if weighed:
+                o += jnp.dot(
+                    w.astype(BF16), kv[first:last, HEAD : 2 * HEAD], preferred_element_type=F32
+                )
+        if scored:
+            peak_buf[m] = top
+        if weighed:
+            slot, m = weighed
+            total = jnp.sum(total, axis=1, keepdims=True)
+            o = (o * (1.0 / total)).astype(BF16).reshape(MEMBERS, 64, HEAD)
+            outs[:, 64 * slot : 64 * slot + 64, m * HEAD : (m + 1) * HEAD] = o
+            return peak, total
+
+    turns = (7, 5, 6, 3, 4, 1, 2, 0)
+
     def attend(p, parts=(0, 1)):
         first, count = rows_of(p)
         parts = [i for i in parts if i < count // 64]
-
         for i in parts:
-            rows = pl.ds(first + 64 * i, 64)
-            found = []
-            for m in (0, 1):
-                cols = slice(m * PART, (m + 1) * PART)
-                q = qs[:, rows, cols].reshape(TILE, PART)
-                s = lax.dot_general(
-                    q, kv[:, cols], (((1,), (1,)), ((), ())), preferred_element_type=F32
-                )
-                near_s = s[:, :LAT_KEYS]
-                far = s[:, LAT_KEYS:] * SCALE2 + lift
-                peak = jnp.maximum(
-                    jnp.max(near_s, axis=1, keepdims=True) * SCALE2,
-                    jnp.max(far, axis=1, keepdims=True),
-                )
-                near_s = jnp.exp2(near_s * SCALE2 - peak)
-                far = jnp.exp2(far - peak)
-                total = jnp.sum(near_s, axis=1, keepdims=True) + jnp.sum(far, axis=1, keepdims=True)
-                o = jnp.dot(
-                    near_s.astype(BF16), kv[:LAT_KEYS, HEAD : 2 * HEAD], preferred_element_type=F32
-                ) + jnp.dot(
-                    far.astype(BF16), kv[LAT_KEYS:, HEAD : 2 * HEAD], preferred_element_type=F32
-                )
-                o = (o / total).astype(BF16).reshape(MEMBERS, 64, HEAD)
-                outs[:, rows, m * HEAD : (m + 1) * HEAD] = o
-                found += [peak, total]
+            slot = first // 64 + i
+            found = beside((slot, 1), (slot, 0))
+            after = turns[turns.index(slot) + 1 :][:1]
+            found += beside((after[0], 0) if after else None, (slot, 1))
             table = jnp.where(
                 column_of == 0,
                 found[0],
                 jnp.where(column_of == 1, found[1], jnp.where(column_of == 2, found[2], found[3])),
             )
             tab[i] = table.reshape(MEMBERS, 64, PART)
+            for j in (2, 1, 3):
+                go(out_copy(p, j, slot))
         if parts[-1] < count // 64 - 1:
             return
         for j in range(MEMBERS):
             second = tab[1, j] if count > 64 else jnp.zeros((64, PART), F32)
             stats[p, j] = jnp.concatenate([tab[0, j], second], axis=0).T[:8, :]
         for j in (2, 1, 3):
-            for copy in out_copies(p, j):
-                go(copy)
-
-    def out_copies(p, j):
-        start, count = rows_of(p)
-        rows = pl.ds(start, count)
-        to = on_queries(j)
-        return (
-            remote(
-                outs.at[j, rows],
-                outs_in.at[4 - j, rows],
-                sent.at[7],
-                outs_r.at[p],
-                to,
-            ),
-            remote(
-                stats.at[p, j],
-                stats_in.at[p, 4 - j],
-                sent.at[8],
-                stats_r.at[p],
-                to,
-            ),
+            go(stats_copy(p, j))
+
+    def out_copy(p, j, slot):
+        rows = pl.ds(64 * slot, 64)
+        return remote(
+            outs.at[j, rows], outs_in.at[4 - j, rows], sent.at[7], outs_r.at[p], on_queries(j)
+        )
+
+    def stats_copy(p, j):
+        return remote(
+            stats.at[p, j], stats_in.at[p, 4 - j], sent.at[8], stats_r.at[p], on_queries(j)
         )
 
     def swap(p):
@@ -606,6 +620,7 @@
                 sum_copy(way, t - 1, h).wait_recv()
                 send_sum(way, t, h, True)
 
+    beside((turns[0], 0), None)
     attend(4)
     attend(3)
     combine(4)
@@ -614,22 +629,23 @@
     multiply(4)
     for way in (0, 1):
         send_sum(way, 1, way, False)
+    combine(3)
     attend(2, (1,))
-    combine(3)
-    attend(1, (0,))
     multiply(3)
     for way in (0, 1):
         send_sum(way, 2, 1 - way, False)
     add_on(2, (0,))
-    attend(1, (1,))
+    attend(1)
     combine(2)
+    multiply(2)
+    add_on(3, (1,))
     attend(0)
-    multiply(2)
-    add_on(3, (1, 0))
+    add_on(3, (0,))
     combine(1)
+    multiply(1)
+    add_on(4, (1,))
     combine(0)
-    multiply(1)
-    add_on(4, (1, 0))
+    add_on(4, (0,))
     multiply(0)
     gathered(1)
     for turn in (1, 0):
@@ -710,6 +726,8 @@
         pltpu.VMEM((KEYS, 2 * HEAD), BF16),
         pltpu.VMEM((4, ROWS, 2 * HEAD), BF16),
         pltpu.VMEM((4, ROWS, 2 * HEAD), BF16),
+        pltpu.VMEM((2, TILE, KEYS), F32),
+        pltpu.VMEM((2, TILE, PART), F32),
         pltpu.VMEM((2, MEMBERS, 64, PART), F32),
         pltpu.VMEM((5, MEMBERS, 8, PART), F32),
         pltpu.VMEM((5, MEMBERS, 8, PART), F32),

time: 85 us -> 84.5 us (level)
  no operation moved by 1% of the time
where the time goes in v4:
time: 84.5 us; the launch traced here: 84.3 us
  Pallas kernels  81.4 us (96%)
  local copies, waits for them, and re-layouts  1.67 us (2%)
  between operations  1.31 us (2%)
    pallas_call x1, Pallas kernels, shards(): pl.pallas_call(body, out_shape=jax.ShapeDtypeStruct(latent.shape, BF16),...  81.4 us

profile of v4, /device:TPU:1, one launch (start us, length us, event | category | flops | bytes accessed | tf_op | source)
XLA Modules:
  0.0 84.3 jit_solution(2125098831029066369)
XLA Ops:
  1.3 81.4 %layer.1 = bf16[32,4096]{1,0:T(8,128)(2,1)} custom-call(bf16[32,4096]{1,0:T(8,128)(2,1)} %latent.1, bf16[32,4096]{1,0:T(8,128)(2,1)} %context.1, f32[32,128]{1,0:T(8,128)} %bitcast.3, f32[32,128]{1,0:T(8,128)} %bitcast.4, bf16[3,256,256]{2,1,0:T(8,128)(2,1)} %modulation.1, bf16[4096,256]{1,0:T(8,128)(2,1)} %query_weight.1, bf16[4096,256]{1,0:T(8,128)(2,1)} %key_weight.1, ...), custom_call_target="tpu_custom_call" | custom-call | tf_op jit(solution)/shard_map/layer/pallas_call | solution.py:753
  82.7 1.7 %copy.20 = bf16[32,4096]{1,0:T(8,128)(2,1)} copy(bf16[32,4096]{1,0:T(8,128)(2,1)} %layer.1) | data formatting | bytes 524288

commit v5 on v4

--- a/solution.py
+++ b/solution.py
@@ -450,9 +450,9 @@
     relay(3, 1)
     hand_on(1)
     slots_in(PASSES[3])
+    hand_on(2)
     step(3)
     relay(4, 0)
-    hand_on(2)
     slots_in(PASSES[4])
     step(4)
     spread(1)

time: 84.5 us -> 87.7 us (1.038)
  Pallas kernels: 81.4 us -> 84.6 us
    pallas_call x1, Pallas kernels: 81.4 us -> 84.6 us  [shards(): pl.pallas_call(body, out_shape=jax.ShapeDtypeStruct(latent.shape, BF16),...]
where the time goes in v5:
time: 87.7 us; the launch traced here: 87.6 us
  Pallas kernels  84.6 us (96%)
  local copies, waits for them, and re-layouts  1.67 us (2%)
  between operations  1.31 us (1%)
    pallas_call x1, Pallas kernels, shards(): pl.pallas_call(body, out_shape=jax.ShapeDtypeStruct(latent.shape, BF16),...  84.6 us

profile of v5, /device:TPU:1, one launch (start us, length us, event | category | flops | bytes accessed | tf_op | source)
XLA Modules:
  0.0 87.6 jit_solution(15544671819135885168)
XLA Ops:
  1.3 84.6 %layer.1 = bf16[32,4096]{1,0:T(8,128)(2,1)} custom-call(bf16[32,4096]{1,0:T(8,128)(2,1)} %latent.1, bf16[32,4096]{1,0:T(8,128)(2,1)} %context.1, f32[32,128]{1,0:T(8,128)} %bitcast.3, f32[32,128]{1,0:T(8,128)} %bitcast.4, bf16[3,256,256]{2,1,0:T(8,128)(2,1)} %modulation.1, bf16[4096,256]{1,0:T(8,128)(2,1)} %query_weight.1, bf16[4096,256]{1,0:T(8,128)(2,1)} %key_weight.1, ...), custom_call_target="tpu_custom_call" | custom-call | tf_op jit(solution)/shard_map/layer/pallas_call | solution.py:753
  85.9 1.7 %copy.20 = bf16[32,4096]{1,0:T(8,128)(2,1)} copy(bf16[32,4096]{1,0:T(8,128)(2,1)} %layer.1) | data formatting | bytes 524288
